TPU v7x, 256 devices: a whole 4x4x8 slice. The times are simulated.
256 devices in a mesh: ep: 128 (over z, y, x), tp: 2 (over core).
Axes of the slice: x: 4, y: 4, z: 8, core: 2. Of those that a mesh axis runs over, the one named last changes fastest.
Arguments:
- tokens: bfloat16 [4096, 2048], P('ep'), may hold values from -6 to 6
- mix_gain: float32 [2048], replicated, may hold values from 0.1 to 1.9
- w_query: bfloat16 [2048, 512], P('ep', 'tp'), may hold values from -0.125 to 0.125
- w_key: bfloat16 [2048, 512], P('ep', 'tp'), may hold values from -0.125 to 0.125
- w_value: bfloat16 [2048, 512], P('ep', 'tp'), may hold values from -0.125 to 0.125
- w_outgate: bfloat16 [2048, 512], P('ep', 'tp'), may hold values from -0.125 to 0.125
- w_igate: bfloat16 [2048, 8], P('ep', 'tp'), may hold values from -0.125 to 0.125
- w_fgate: bfloat16 [2048, 8], P('ep', 'tp'), may hold values from -0.125 to 0.125
- igate_bias: float32 [8], P('tp'), may hold values from -2 to 1
- fgate_bias: float32 [8], P('tp'), may hold values from 0 to 4
- head_gain: float32 [512], P('tp'), may hold values from 0.1 to 1.9
- w_out: bfloat16 [512, 2048], P('tp', 'ep'), may hold values from -0.25 to 0.25
- state_matrix: float32 [4096, 8, 64, 64], P('ep', 'tp'), may hold values from -2.4 to 2.4
- state_norm: float32 [4096, 8, 64], P('ep', 'tp'), may hold values from -2.4 to 2.4
- state_max: float32 [4096, 8], P('ep', 'tp'), may hold values from -4 to 4
- ffn_gain: float32 [2048], replicated, may hold values from 0.1 to 1.9
- w_expert_gate: bfloat16 [128, 2048, 1408], P('ep', None, 'tp'), may hold values from -0.125 to 0.125
- w_expert_up: bfloat16 [128, 2048, 1408], P('ep', None, 'tp'), may hold values from -0.125 to 0.125
- w_expert_down: bfloat16 [128, 1408, 2048], P('ep', 'tp'), may hold values from -0.15625 to 0.15625
- routes: int32 [4096, 3], P('ep'), may hold values from 0 to 127, all different within a row; in each aligned block of 32 rows (0 to 31, 32 to 63, ...) at most 2 rows name the same one
- route_weights: float32 [4096, 3], P('ep'), may hold values from 0.2 to 1
Outputs:
- mixed: bfloat16 [4096, 2048], P('ep')
- new_matrix: float32 [4096, 8, 64, 64], P('ep', 'tp')
- new_norm: float32 [4096, 8, 64], P('ep', 'tp')
- new_max: float32 [4096, 8], P('ep', 'tp')
Inputs may be any that keep to these rules, and one draw needn't show every extreme that they name: `routes`: each row names 3 different experts. Among the rows of one device, no expert is named by more than 2 rows, a bound that some block reaches.
All inputs are finite; a program needn't handle non-finite values.
Results may differ from a plain program's by a relative error of at most 0.017.
Values may be sent and summed in bfloat16 or wider, within the bound.
A program may use at most 128 MiB of HBM per device.

v0:
```python
import jax
import jax.numpy as jnp
from jax import lax
from jax.sharding import Mesh
from jax.sharding import PartitionSpec as P

EP = ("ep_0", "ep_1", "ep_2")


def sent_together(arrays, axis, dim, along):
    both = jnp.concatenate(arrays, axis=along)
    filled, at, done = (lax.all_gather(both, axis, axis=dim, tiled=True), 0, [])
    for a in arrays:
        done.append(lax.slice_in_dim(filled, at, at + a.shape[along], axis=along))
        at += a.shape[along]
    return tuple(done)


def gathered_by_axis(value, axes, dim):
    if not axes:
        return value
    nearer = lax.all_gather(value, axes[-1], axis=dim, tiled=True)
    return gathered_by_axis(nearer, axes[:-1], dim)


def sent_to_all(value, axis):
    copies = jnp.broadcast_to(value, (lax.axis_size(axis), *value.shape))
    return lax.all_to_all(copies, axis, split_axis=0, concat_axis=0, tiled=True)


def taken_together(value, axis):
    return sent_to_all(value, axis).astype(jnp.float32).sum(axis=0)


def rms_scale(values_in, gain_vec):
    widened = values_in.astype(jnp.float32)
    return (
        widened * lax.rsqrt(jnp.mean(widened * widened, axis=-1, keepdims=True) + 1e-06) * gain_vec
    )


def memory_cell(
    query,
    key_row,
    value_row,
    outgate,
    input_pre,
    forget_pre,
    head_gain,
    state_matrix,
    state_norm,
    state_max,
):
    seq_rows, head_count = input_pre.shape
    head_size = query.shape[1] // head_count
    query_heads = query.astype(jnp.float32).reshape(seq_rows, head_count, head_size)
    key_heads = key_row.astype(jnp.float32).reshape(
        seq_rows, head_count, head_size
    ) * head_size ** (-0.5)
    value_heads = value_row.astype(jnp.float32).reshape(seq_rows, head_count, head_size)
    log_forget = jax.nn.log_sigmoid(forget_pre)
    new_max = jnp.maximum(log_forget + state_max, input_pre)
    keep_old = jnp.exp(log_forget + state_max - new_max)
    keep_new = jnp.exp(input_pre - new_max)
    new_matrix = (
        keep_old[:, :, None, None] * state_matrix
        + keep_new[:, :, None, None] * value_heads[:, :, :, None] * key_heads[:, :, None, :]
    )
    new_norm = keep_old[:, :, None] * state_norm + keep_new[:, :, None] * key_heads
    numerator = jnp.einsum("bhvd,bhd->bhv", new_matrix, query_heads)
    denominator = jnp.sum(new_norm * query_heads, axis=-1)
    cell_read = numerator / jnp.maximum(jnp.abs(denominator), jnp.exp(-new_max))[:, :, None]
    centered = cell_read - jnp.mean(cell_read, axis=-1, keepdims=True)
    variance = jnp.mean(centered * centered, axis=-1, keepdims=True)
    scaled_cell = (centered * lax.rsqrt(variance + 1e-06)).reshape(seq_rows, head_count * head_size)
    cell_out = (scaled_cell * head_gain * jax.nn.sigmoid(outgate.astype(jnp.float32))).astype(
        jnp.bfloat16
    )
    return (cell_out, new_matrix, new_norm, new_max)


def body(
    tokens,
    mix_gain,
    w_query,
    w_key,
    w_value,
    w_outgate,
    w_igate,
    w_fgate,
    igate_bias,
    fgate_bias,
    head_gain,
    w_out,
    state_matrix,
    state_norm,
    state_max,
    ffn_gain,
    w_expert_gate,
    w_expert_up,
    w_expert_down,
    routes,
    route_weights,
):
    seq_rows, width = tokens.shape
    normed = rms_scale(tokens, mix_gain).astype(jnp.bfloat16)
    pieces = sent_together((w_query, w_key, w_value, w_outgate, w_igate, w_fgate), EP, 0, 1)
    projected = tuple(
        (jnp.dot(normed, shard_piece, preferred_element_type=jnp.float32) for shard_piece in pieces)
    )
    query = projected[0].astype(jnp.bfloat16)
    key_row = projected[1].astype(jnp.bfloat16)
    value_row = projected[2].astype(jnp.bfloat16)
    outgate = projected[3].astype(jnp.bfloat16)
    input_pre = projected[4] + igate_bias
    forget_pre = projected[5] + fgate_bias
    cell_out, new_matrix, new_norm, new_max = memory_cell(
        query,
        key_row,
        value_row,
        outgate,
        input_pre,
        forget_pre,
        head_gain,
        state_matrix,
        state_norm,
        state_max,
    )
    partial_out = jnp.dot(
        cell_out, gathered_by_axis(w_out, EP, 1), preferred_element_type=jnp.float32
    )
    attended = taken_together(partial_out.astype(jnp.bfloat16), "tp").astype(jnp.float32)
    resid = (tokens.astype(jnp.float32) + attended).astype(jnp.bfloat16)
    normed_two = rms_scale(resid, ffn_gain).astype(jnp.bfloat16)
    ep_count = lax.axis_size(EP)
    local_experts = w_expert_gate.shape[0]
    expert_total = local_experts * ep_count
    top_count = routes.shape[1]
    capacity = max(2, 2 * seq_rows * top_count // expert_total)
    flat_routes = routes.reshape(-1)
    onehot = (flat_routes[:, None] == jnp.arange(expert_total, dtype=jnp.int32)[None, :]).astype(
        jnp.int32
    )
    earlier = jnp.cumsum(onehot, axis=0, dtype=jnp.int32) - onehot
    slots = jnp.sum(onehot * earlier, axis=1, dtype=jnp.int32)
    targets = flat_routes * capacity + slots
    dispatch = (
        targets[:, None] == jnp.arange(expert_total * capacity, dtype=jnp.int32)[None, :]
    ).astype(jnp.bfloat16)
    route_rows = jnp.repeat(normed_two, top_count, axis=0)
    outgoing = jnp.einsum(
        "rs,rd->sd", dispatch, route_rows, preferred_element_type=jnp.float32
    ).astype(jnp.bfloat16)
    outgoing = outgoing.reshape(expert_total, capacity, width)
    received = lax.all_to_all(outgoing, EP, split_axis=0, concat_axis=0, tiled=True)
    slot_count = received.shape[1]
    regrouped = received.reshape(ep_count, local_experts, slot_count, width)
    gate_pre = jnp.einsum(
        "nxcd,xdf->nxcf", regrouped, w_expert_gate, preferred_element_type=jnp.float32
    )
    up_pre = jnp.einsum(
        "nxcd,xdf->nxcf", regrouped, w_expert_up, preferred_element_type=jnp.float32
    )
    hidden = (jax.nn.silu(gate_pre) * up_pre).astype(jnp.bfloat16)
    partial_down = jnp.einsum(
        "nxcf,xfd->nxcd", hidden, w_expert_down, preferred_element_type=jnp.float32
    )
    expert_sum = taken_together(partial_down.astype(jnp.bfloat16), "tp").astype(jnp.float32)
    finished = expert_sum.astype(jnp.bfloat16).reshape(ep_count * local_experts, slot_count, width)
    returned = lax.all_to_all(finished, EP, split_axis=0, concat_axis=0, tiled=True)
    picked = jnp.dot(
        dispatch,
        returned.reshape(expert_total * capacity, width),
        preferred_element_type=jnp.float32,
    )
    weighted = jnp.sum(
        picked.reshape(seq_rows, top_count, width) * route_weights[:, :, None], axis=1
    )
    mixed = (resid.astype(jnp.float32) + weighted).astype(jnp.bfloat16)
    return (mixed, new_matrix, new_norm, new_max)


def solution(mesh):
    torus = Mesh(mesh.devices.reshape(8, 4, 4, mesh.shape["tp"]), ("ep_0", "ep_1", "ep_2", "tp"))
    placed = (
        P(EP, None),
        P(),
        P(EP, "tp"),
        P(EP, "tp"),
        P(EP, "tp"),
        P(EP, "tp"),
        P(EP, "tp"),
        P(EP, "tp"),
        P("tp"),
        P("tp"),
        P("tp"),
        P("tp", EP),
        P(EP, "tp", None, None),
        P(EP, "tp", None),
        P(EP, "tp"),
        P(),
        P(EP, None, "tp"),
        P(EP, None, "tp"),
        P(EP, "tp", None),
        P(EP, None),
        P(EP, None),
    )
    return jax.shard_map(
        body,
        mesh=torus,
        in_specs=placed,
        out_specs=(P(EP, None), P(EP, "tp", None, None), P(EP, "tp", None), P(EP, "tp")),
        check_vma=False,
    )
```

profile of v0, /device:TPU:1, one launch (start us, length us, event | category | flops | bytes accessed | tf_op | source)
XLA Modules:
  0.0 300.7 jit_solution(6747754520496380764)
XLA Ops:
  7.2 0.0 copy-start
  7.2 0.0 all-gather.3.cloned.1.call-start
  7.3 0.9 copy.96
  8.2 0.8 copy.97
  8.9 1.4 concatenate.3
  10.4 0.0 all-gather.3.cloned.1.call-update
  10.4 0.0 all-gather.5.cloned.1.call-start
  10.5 10.4 %all_gather.13 = bf16[256,64]{0,1:T(8,128)(2,1)S(1)} all-gather(bf16[256,16]{0,1:T(8,128)(2,1)} %param.32), channel_id=1, replica_groups=mesh['ep_0'=8,'ep_1'=4,'ep_2'=4,'tp'=2] {'ep_2'}, dimensions={1}, use_global_device_ids=true | all-gather | bytes 40960 | tf_op jit(solution)/shard_map/all_gather | solution.py:22
  20.9 10.4 %all_gather.14 = bf16[256,256]{0,1:T(8,128)(2,1)} all-gather(bf16[256,64]{0,1:T(8,128)(2,1)S(1)} %all_gather.13), channel_id=1, replica_groups=mesh['ep_0'=8,'ep_1'=4,'ep_2'=4,'tp'=2] {'ep_1'}, dimensions={1}, use_global_device_ids=true | all-gather | bytes 163840 | tf_op jit(solution)/shard_map/all_gather | solution.py:22
  31.2 0.0 all-gather.5.cloned.1.call-update
  31.3 1.0 fusion.52
  32.3 0.8 copy.104
  33.1 0.1 eq.50
  33.2 0.1 fusion.64
  33.3 0.1 reduce_window_sum.11
  33.4 0.2 select_reduce_fusion
  33.6 95.9 %all-gather.3.cloned.1.call-done = bf16[2048,1032]{1,0:T(8,128)(2,1)} async-done(((bf16[16,1032]{1,0:T(8,128)(2,1)}), bf16[2048,1032]{1,0:T(8,128)(2,1)}) %all-gather.3.cloned.1.call-update) | async-done | bytes 4227088 | tf_op jit(solution)/shard_map/all_gather | solution.py:12
  129.5 1.7 fusion.69
  131.2 1.4 broadcast_multiply_fusion.3
  132.6 0.0 copy-start.8
  132.7 0.1 copy.98
  132.8 0.1 copy.101
  132.9 0.1 copy.99
  132.9 1.6 convolution_convert_fusion.3
  134.6 0.1 reshape.148
  134.7 1.6 fusion.33
  136.3 0.1 reshape.158
  136.5 1.5 fusion.32
  138.0 0.1 reshape.160
  138.1 0.8 multiply_reduce_fusion.1
  138.9 0.1 copy.102
  139.0 0.1 reshape.168
  139.1 0.1 copy.103
  139.2 3.7 %multiply_add_fusion = f32[32,4,64,64]{3,2,1,0:T(8,128)S(1)} fusion(f32[32,4,64,64]{3,2,1,0:T(8,128)} %param.33, f32[32,4,64]{2,1,0:T(4,128)S(1)} %get-tuple-element.13, f32[32,4,64]{2,1,0:T(4,128)S(1)} %get-tuple-element.14, f32[32,4]{1,0:T(8,128)S(1)} %copy.98), kind=kLoop, calls=%fused_computation | loop fusion | flops 1572864 | bytes 4260352 | tf_op jit(solution)/shard_map/add | solution.py:66
  142.9 2.0 copy-done.1
  144.9 1.2 fusion.83
  146.1 0.2 fusion.82
  146.3 0.2 multiply_reduce_fusion
  146.5 0.1 subtract_multiply_fusion
  146.7 0.1 reshape.150
  146.8 18.7 %all-gather.5.cloned.1.call-done = bf16[256,2048]{0,1:T(8,128)(2,1)} async-done(((bf16[256,256]{0,1:T(8,128)(2,1)}), bf16[256,2048]{0,1:T(8,128)(2,1)}) %all-gather.5.cloned.1.call-update) | async-done | bytes 1048592 | tf_op jit(solution)/shard_map/all_gather | solution.py:22
  165.4 2.4 convolution_convert_fusion.1
  167.9 9.3 %all_to_all.20 = bf16[2,32,2048]{2,1,0:T(8,128)(2,1)S(1)} all-to-all(bf16[2,32,2048]{2,1,0:T(8,128)(2,1)S(1)} %broadcast_in_dim.6), channel_id=1, replica_groups=mesh['ep_0'=8,'ep_1'=4,'ep_2'=4,'tp'=2] {'tp'}, dimensions={0} | all-to-all | bytes 524288 | tf_op jit(solution)/shard_map/all_to_all | solution.py:28
  177.3 0.2 fusion.56
  177.4 0.1 fusion.58
  177.5 0.2 broadcast_in_dim.7
  177.8 1.1 reshape.151
  178.9 2.5 convolution_convert_fusion
  181.4 2.5 reshape.152
  183.9 40.0 %all_to_all.21 = bf16[128,2,2048]{2,1,0:T(2,128)(2,1)S(1)} all-to-all(bf16[128,2,2048]{2,1,0:T(2,128)(2,1)} %reshape.152), channel_id=1, replica_groups=mesh['ep_0'=8,'ep_1'=4,'ep_2'=4,'tp'=2] {'ep_0','ep_1','ep_2'}, dimensions={0} | all-to-all | bytes 2097152 | tf_op jit(solution)/shard_map/all_to_all | solution.py:155
  223.9 1.0 copy-done.3
  224.9 4.0 %fusion.9 = f32[128,1,2,704]{0,3,2,1:T(8,128)} fusion(bf16[1,2048,704]{1,2,0:T(8,128)(2,1)} %param.37, bf16[128,2,2048]{2,1,0:T(2,128)(2,1)S(1)} %all_to_all.21), kind=kOutput, calls=%fused_computation.11 | convolution fusion | flops 738197504 | bytes 4653056 | tf_op jit(solution)/shard_map/nxcd,xdf->nxcf/dot_general | solution.py:158
  228.9 6.6 %fusion.6 = bf16[128,2,2048]{2,0,1:T(8,128)(2,1)} fusion(bf16[1,704,2048]{2,1,0:T(8,128)(2,1)S(1)} %copy-done, bf16[1,2048,704]{1,2,0:T(8,128)(2,1)} %param.38, bf16[128,2,2048]{2,1,0:T(2,128)(2,1)} %copy-done.3, f32[128,1,2,704]{0,3,2,1:T(8,128)} %fusion.9), kind=kOutput, calls=%fused_computation.8 | convolution fusion | flops 1478000640 | bytes 8585216 | tf_op jit(solution)/shard_map/nxcf,xfd->nxcd/dot_general | solution.py:165
  235.5 1.5 broadcast_in_dim.8
  237.1 9.1 %all_to_all.22 = bf16[2,128,1,2,2048]{4,1,3,2,0:T(8,128)(2,1)} all-to-all(bf16[2,128,1,2,2048]{4,1,3,2,0:T(8,128)(2,1)S(1)} %broadcast_in_dim.8), channel_id=1, replica_groups=mesh['ep_0'=8,'ep_1'=4,'ep_2'=4,'tp'=2] {'tp'}, dimensions={0} | all-to-all | bytes 4194304 | tf_op jit(solution)/shard_map/all_to_all | solution.py:28
  246.1 3.3 %reduce_sum.94 = bf16[128,2,2048]{2,0,1:T(8,128)(2,1)} reduce(bf16[2,128,1,2,2048]{4,1,3,2,0:T(8,128)(2,1)} %all_to_all.22, bf16[]{:T(256)} %constant.31.clone.1), dimensions={0,2}, to_apply=%region_8.9 | reduce | flops 524288 | bytes 3145730 | tf_op jit(solution)/shard_map/reduce_sum | solution.py:32
  249.4 3.3 %copy.108 = bf16[128,2,2048]{2,1,0:T(2,128)(2,1)} copy(bf16[128,2,2048]{2,0,1:T(8,128)(2,1)} %reduce_sum.94) | data formatting | bytes 2097152 | tf_op jit(solution)/shard_map/reduce_sum | solution.py:32
  252.8 7.3 %all-to-all-start.3 = ((bf16[128,2,2048]{2,1,0:T(2,128)(2,1)}), bf16[128,2,2048]{2,1,0:T(2,128)(2,1)}, u32[]{:S(2)}, u32[]{:S(2)}) async-start(bf16[128,2,2048]{2,1,0:T(2,128)(2,1)} %copy.108), calls=%async_computation.3 | async-start | bytes 2097152 | tf_op jit(solution)/shard_map/all_to_all | solution.py:170
  260.1 0.1 reduce_sum.92
  260.2 0.1 copy.105
  260.3 29.0 %all-to-all-done.3 = bf16[128,2,2048]{2,1,0:T(2,128)(2,1)} async-done(((bf16[128,2,2048]{2,1,0:T(2,128)(2,1)}), bf16[128,2,2048]{2,1,0:T(2,128)(2,1)}, u32[]{:S(2)}, u32[]{:S(2)}) %all-to-all-start.3) | async-done | bytes 1048608 | tf_op jit(solution)/shard_map/all_to_all | solution.py:170
  289.3 2.3 reshape.166
  291.5 1.6 fusion.21
  293.1 0.7 fusion.59
  (28 shorter events, 0.2 us)
Async XLA Ops:
  7.2 221.7 %copy-start = (bf16[1,704,2048]{2,1,0:T(8,128)(2,1)S(1)}, bf16[1,704,2048]{2,1,0:T(8,128)(2,1)}, u32[]{:S(2)}) copy-start(bf16[1,704,2048]{2,1,0:T(8,128)(2,1)} %param.39) | copy-start | bytes 8650756
  7.2 129.3 %copy-start.2 = (bf16[32,2048]{1,0:T(8,128)(2,1)S(1)}, bf16[32,2048]{1,0:T(8,128)(2,1)}, u32[]{:S(2)}) copy-start(bf16[32,2048]{1,0:T(8,128)(2,1)} %param.21) | copy-start | bytes 393220
  7.2 129.3 %copy-start.5 = (f32[2048]{0:T(1024)S(1)}, f32[2048]{0:T(1024)}, u32[]{:S(2)}) copy-start(f32[2048]{0:T(1024)} %param.22) | copy-start | bytes 24580
  7.2 130.9 %copy-start.4 = (f32[32,4,64]{2,1,0:T(4,128)S(1)}, f32[32,4,64]{2,1,0:T(4,128)}, u32[]{:S(2)}) copy-start(f32[32,4,64]{2,1,0:T(4,128)} %param.34) | copy-start | bytes 98308
  7.2 122.3 %all-gather.3.cloned.1.call-start = ((), (), s32[]{:S(2)}) async-start(), calls=%async_computation.4 | async-start | bytes 4755456 | tf_op jit(solution)/shard_map/all_gather | solution.py:12
  10.4 155.0 %all-gather.5.cloned.1.call-start = ((), (), s32[]{:S(2)}) async-start(), calls=%async_computation.5 | async-start | bytes 1179648 | tf_op jit(solution)/shard_map/all_gather | solution.py:22
  132.6 10.3 %copy-start.8 = (f32[32,4]{0,1:T(4,128)}, f32[32,4]{0,1:T(4,128)S(1)}, u32[]{:S(2)}) copy-start(f32[32,4]{0,1:T(4,128)S(1)} %get-tuple-element.12) | copy-start | bytes 1540
  142.9 2.0 copy-start.1
  144.9 20.5 %copy-start.10 = (f32[256]{0:T(256)S(1)}, f32[256]{0:T(256)}, u32[]{:S(2)}) copy-start(f32[256]{0:T(256)} %param.31) | copy-start | bytes 3076
  144.9 32.5 %copy-start.6 = (f32[2048]{0:T(1024)S(1)}, f32[2048]{0:T(1024)}, u32[]{:S(2)}) copy-start(f32[2048]{0:T(1024)} %param.36) | copy-start | bytes 24580
  223.9 1.0 copy-start.3
  246.1 14.2 %copy-start.7 = (s32[32,3]{0,1:T(4,128)S(1)}, s32[32,3]{0,1:T(4,128)}, u32[]{:S(2)}) copy-start(s32[32,3]{0,1:T(4,128)} %param.40) | copy-start | bytes 1156
  246.1 45.4 %copy-start.9 = (f32[32,3]{0,1:T(4,128)S(1)}, f32[32,3]{0,1:T(4,128)}, u32[]{:S(2)}) copy-start(f32[32,3]{0,1:T(4,128)} %param.41) | copy-start | bytes 1156
  252.8 36.5 %all-to-all-start.3 = ((bf16[128,2,2048]{2,1,0:T(2,128)(2,1)}), bf16[128,2,2048]{2,1,0:T(2,128)(2,1)}, u32[]{:S(2)}, u32[]{:S(2)}) async-start(bf16[128,2,2048]{2,1,0:T(2,128)(2,1)} %copy.108), calls=%async_computation.3 | async-start | bytes 2097152 | tf_op jit(solution)/shard_map/all_to_all | solution.py:170
Sparse Core Ops, SparseCore 0:
  12.4 117.0 all-gather.2
  131.3 34.1 all-gather.4
where the time goes:
time: 302 us; the launch traced here: 301 us
  waiting for transfers between devices  144 us (48%)
  blocking collectives  79.1 us (26%)
  matrix products  26.3 us (9%)
  local copies, waits for them, and re-layouts  19.2 us (6%)
  between operations  14.3 us (5%)
  other arithmetic  10.8 us (4%)
  starting transfers between devices  7.4 us (2%)
    all_gather x1, waiting for transfers between devices, sent_together(): filled, at, done = (lax.all_gather(both, axis, axis=dim, tiled=True), 0, [])  95.9 us
    all_to_all x1, blocking collectives, body(): lax.all_to_all(outgoing, EP, split_axis=0, concat_axis=0, tiled=True)  40 us
    all_to_all x1, waiting for transfers between devices, body(): lax.all_to_all(finished, EP, split_axis=0, concat_axis=0, tiled=True)  29 us
    all_gather x2, blocking collectives, gathered_by_axis(): nearer = lax.all_gather(value, axes[-1], axis=dim, tiled=True)  20.8 us
    all_gather x1, waiting for transfers between devices, gathered_by_axis(): nearer = lax.all_gather(value, axes[-1], axis=dim, tiled=True)  18.7 us
    all_to_all x2, blocking collectives, sent_to_all(): return lax.all_to_all(copies, axis, split_axis=0, concat_axis=0, tiled=True)  18.3 us
    dot_general x5, matrix products, body(): jnp.dot(normed, shard_piece, preferred_element_type=jnp.float32)  7.95 us
    all_to_all x1, starting transfers between devices, body(): lax.all_to_all(finished, EP, split_axis=0, concat_axis=0, tiled=True)  7.32 us
  transfers between devices with their start and end apart: 3, of which 3 were waited for; matrix products, arithmetic and copies ran while one was open for 6% of the time, Pallas kernels for 0%

commit v1 on v0

v1 whole, which is shorter than its diff:
```python
import jax
import jax.numpy as jnp
from jax import lax
from jax.experimental import pallas as pl
from jax.experimental.pallas import tpu as pltpu
from jax.sharding import Mesh
from jax.sharding import PartitionSpec as P

EP = ("ep_0", "ep_1", "ep_2")
NZ, NY, NX = 8, 4, 4
NP = NY * NX
D, HALF = 2048, 1024
DE = 704
ROWS = 32
MESH = pl.DeviceIdType.MESH
F32, BF16 = jnp.float32, jnp.bfloat16


def whereami():
    return (
        lax.axis_index("ep_0"),
        lax.axis_index("ep_1"),
        lax.axis_index("ep_2"),
        lax.axis_index("tp"),
    )


def push(src, dst, send_sem, recv_sem, to):
    return pltpu.make_async_remote_copy(
        src_ref=src,
        dst_ref=dst,
        send_sem=send_sem,
        recv_sem=recv_sem,
        device_id=to,
        device_id_type=MESH,
    )


def nt_dot(a, b):
    return lax.dot_general(a, b, (((1,), (1,)), ((), ())), preferred_element_type=F32)


def nn_dot(a, b):
    return jnp.dot(a, b, preferred_element_type=F32)


def rms_scale(values, gain):
    return values * lax.rsqrt(jnp.mean(values * values, axis=-1, keepdims=True) + 1e-06) * gain


def gather_kernel(
    tok_ref, gain_ref, wp_ref, wo_ref,
    proj_ref, gates_ref, wof_ref,
    nall, wst, gsum, wfull, gt, woz, res,
    n_s, n_r, f_s, f_r, w_s, w_r, o_s, o_r, x_s, x_r, g_s, g_r, v_s, v_r, p_s, p_r,
):
    z, y, x, c = whereami()
    yx = y * NX + x
    half = pl.ds(pl.multiple_of(c * HALF, HALF), HALF)
    other = pl.ds(pl.multiple_of((1 - c) * HALF, HALF), HALF)
    partner = (z, y, x, 1 - c)

    def zpeer(d):
        return (z + d) % NZ

    def ppeer(d):
        yt, xt = (y + d // NX) % NY, (x + d % NX) % NX
        return yt, xt, yt * NX + xt

    barrier = pltpu.get_barrier_semaphore()
    for d in range(1, NZ):
        pl.semaphore_signal(barrier, 1, device_id=(zpeer(d), y, x, c), device_id_type=MESH)

    def greet(d, carry):
        yt, xt, _ = ppeer(d)
        pl.semaphore_signal(barrier, 1, device_id=(z, yt, xt, c), device_id_type=MESH)
        return carry

    lax.fori_loop(1, NP, greet, 0)
    pl.semaphore_signal(barrier, 1, device_id=partner, device_id_type=MESH)

    nall[z] = rms_scale(tok_ref[...].astype(F32), gain_ref[...]).astype(BF16)
    wst[z] = wp_ref[z]
    woz[z] = wo_ref[...]

    pl.semaphore_wait(barrier, NZ - 1 + NP - 1 + 1)

    order = (4, 3, 5, 2, 6, 1, 7)

    def w_send(d):
        zt = zpeer(d)
        return push(wp_ref.at[zt], wst.at[z], w_s.at[zt], w_r.at[z], (zt, y, x, c))

    def o_send(d):
        zt = zpeer(d)
        return push(wo_ref, woz.at[z], o_s.at[zt], o_r.at[z], (zt, y, x, c))

    def n_send(d):
        zt = zpeer(d)
        return push(nall.at[z, :, half], nall.at[z, :, half], n_s.at[zt], n_r.at[z], (zt, y, x, c))

    for d in order:
        w_send(d).start()
    for d in order:
        o_send(d).start()
    for d in order:
        n_send(d).start()

    def arrived(src, dst, recv_sem):
        push(src, dst, recv_sem, recv_sem, partner).wait_recv()

    for d in range(1, NZ):
        zs = zpeer(d)
        arrived(wst.at[zs], wst.at[zs], w_r.at[zs])
    total = wst[0, 16:32, :].astype(F32)
    for k in range(1, NZ):
        total = total + wst[k, 16:32, :].astype(F32)
    gsum[...] = total.astype(BF16)
    gt[yx] = gsum[...]
    for k in range(NZ):
        wfull[k, yx] = wst[k, 0:16, :]

    def x_send(d):
        yt, xt, yxt = ppeer(d)
        return push(wst.at[:, 0:16, :], wfull.at[:, yx], x_s.at[yxt], x_r.at[yx], (z, yt, xt, c))

    def g_send(d):
        yt, xt, yxt = ppeer(d)
        return push(gsum, gt.at[yx], g_s.at[yxt], g_r.at[yx], (z, yt, xt, c))

    def v_send(d):
        yt, xt, yxt = ppeer(d)
        return push(woz, wof_ref.at[:, yx], v_s.at[yxt], v_r.at[yx], (z, yt, xt, c))

    def start_xg(d, carry):
        x_send(d).start()
        g_send(d).start()
        return carry

    lax.fori_loop(1, NP, start_xg, 0)

    for d in range(1, NZ):
        zs = zpeer(d)
        arrived(woz.at[zs], woz.at[zs], o_r.at[zs])
    for k in range(NZ):
        wof_ref[k, yx] = woz[k]

    def start_v(d, carry):
        v_send(d).start()
        return carry

    lax.fori_loop(1, NP, start_v, 0)

    def f_send(zs):
        return push(nall.at[zs, :, half], nall.at[zs, :, half], f_s.at[zs], f_r.at[zs], partner)

    for d in (1, 7, 2, 6, 3, 5, 4):
        zs = zpeer(d)
        arrived(nall.at[zs, :, half], nall.at[zs, :, half], n_r.at[zs])
        f_send(zs).start()
    for d in (1, 7, 2, 6, 3, 5, 4):
        zs = zpeer(d)
        arrived(nall.at[zs, :, other], nall.at[zs, :, other], f_r.at[zs])

    def wait_xg(d, carry):
        _, _, s = ppeer(d)
        arrived(wfull.at[:, s], wfull.at[:, s], x_r.at[s])
        arrived(gt.at[s], gt.at[s], g_r.at[s])
        return carry

    lax.fori_loop(1, NP, wait_xg, 0)

    every = nn_dot(nall[...].reshape(NZ * ROWS, D), wfull[...].reshape(D, 128))
    res[...] = every.astype(BF16).reshape(NZ, ROWS, 128)
    proj_ref[z] = res[z]

    def p_send(d):
        zt = zpeer(d)
        return push(res.at[zt], proj_ref.at[z], p_s.at[zt], p_r.at[z], (zt, y, x, c))

    for d in order:
        p_send(d).start()

    mine = nall[z]
    stacked = jnp.concatenate([mine[:, 256 * k:256 * (k + 1)] for k in range(NZ)], axis=0)
    gp = nn_dot(stacked, gt[...].reshape(256, 128))
    group = lax.broadcasted_iota(jnp.int32, (ROWS, 128), 1) // 8
    acc = jnp.zeros((ROWS, 128), F32)
    for k in range(NZ):
        acc = acc + jnp.where(group == k, gp[ROWS * k:ROWS * (k + 1)], 0.0)
    for shift in (64, 32, 16, 8):
        acc = acc + pltpu.roll(acc, shift, 1)
    gates_ref[...] = acc

    for d in range(1, NZ):
        zs = zpeer(d)
        arrived(proj_ref.at[zs], proj_ref.at[zs], p_r.at[zs])

    def wait_v(d, carry):
        _, _, s = ppeer(d)
        arrived(wof_ref.at[:, s], wof_ref.at[:, s], v_r.at[s])
        return carry

    lax.fori_loop(1, NP, wait_v, 0)

    for d in range(1, NZ):
        w_send(d).wait_send()
        o_send(d).wait_send()
        n_send(d).wait_send()
        f_send(zpeer(d)).wait_send()
        p_send(d).wait_send()

    def sent(d, carry):
        x_send(d).wait_send()
        g_send(d).wait_send()
        v_send(d).wait_send()
        return carry

    lax.fori_loop(1, NP, sent, 0)


def gather(tokens, mix_gain, wp, wo_t):
    dma = pltpu.SemaphoreType.DMA
    vm = pl.BlockSpec(memory_space=pltpu.VMEM)
    sems = []
    for count in (NZ, NZ, NZ, NZ, NP, NP, NP, NZ):
        sems += [dma((count,)), dma((count,))]
    return pl.pallas_call(
        gather_kernel,
        name="gather",
        out_shape=(
            jax.ShapeDtypeStruct((NZ, ROWS, 128), BF16),
            jax.ShapeDtypeStruct((ROWS, 128), F32),
            jax.ShapeDtypeStruct((NZ, NP, 16, 256), BF16),
        ),
        in_specs=[vm] * 4,
        out_specs=(vm, vm, vm),
        scratch_shapes=[
            pltpu.VMEM((NZ, ROWS, D), BF16),
            pltpu.VMEM((NZ, 32, 128), BF16),
            pltpu.VMEM((16, 128), BF16),
            pltpu.VMEM((NZ, NP, 16, 128), BF16),
            pltpu.VMEM((NP, 16, 128), BF16),
            pltpu.VMEM((NZ, 16, 256), BF16),
            pltpu.VMEM((NZ, ROWS, 128), BF16),
            *sems,
        ],
        compiler_params=pltpu.CompilerParams(
            collective_id=0, has_side_effects=True, vmem_limit_bytes=32 << 20
        ),
    )(tokens, mix_gain.reshape(1, D), wp, wo_t)


def expert_kernel(
    cell_ref, tok_ref, gain_ref, wof_ref, crow_ref, ccol_ref, wcol_ref, wg_hbm, wu_hbm, wd_hbm,
    mixed_ref,
    p_my, p_ot, resid, ntwo, amat, whi, wlo, outt, rcv, xf, xm, wg, wu, wd, hid, pd, pd_ot, back, ret,
    ld, q_s, q_r, d_s, d_r, h_s, h_r, k_s, k_r, b_s, b_r, m_s, m_r,
):
    z, y, x, c = whereami()
    yx = y * NX + x
    me = z * NP + yx
    partner = (z, y, x, 1 - c)
    half = pl.ds(pl.multiple_of(c * HALF, HALF), HALF)
    other = pl.ds(pl.multiple_of((1 - c) * HALF, HALF), HALF)

    loads = [
        pltpu.make_async_copy(wg_hbm.at[0], wg, ld.at[0]),
        pltpu.make_async_copy(wu_hbm.at[0], wu, ld.at[1]),
        pltpu.make_async_copy(wd_hbm.at[0], wd, ld.at[2]),
    ]
    for load in loads:
        load.start()

    def place(i, j):
        zt = (z + i) % NZ
        yt, xt = (y + j // NX) % NY, (x + j % NX) % NX
        return (zt, yt, xt, c), zt * NP + yt * NX + xt

    def over_peers(body):
        def outer(i, carry):
            def inner(j, carry2):
                body(i, j)
                return carry2

            lax.fori_loop(jnp.where(i == 0, 1, 0), NP, inner, 0)
            return carry

        lax.fori_loop(0, NZ, outer, 0)

    barrier = pltpu.get_barrier_semaphore()

    def greet(i, j):
        to, _ = place(i, j)
        pl.semaphore_signal(barrier, 1, device_id=to, device_id_type=MESH)

    over_peers(greet)
    pl.semaphore_signal(barrier, 1, device_id=partner, device_id_type=MESH)

    part = nt_dot(cell_ref[...], wof_ref[...].reshape(D, 256))
    p_my[...] = part.astype(BF16)

    def build_a(i, carry):
        at = pl.ds(pl.multiple_of(i * 256, 256), 256)
        row = lax.broadcasted_iota(jnp.int32, (256, 256), 0) + i * 256
        hit = (row == crow_ref[0:1, :]) | (row == crow_ref[1:2, :]) | (row == crow_ref[2:3, :])
        amat[at, :] = jnp.where(hit, 1.0, 0.0).astype(BF16)
        col = lax.broadcasted_iota(jnp.int32, (256, 256), 1) + i * 256
        weight = jnp.zeros((256, 256), F32)
        for k in range(3):
            weight = weight + jnp.where(col == ccol_ref[:, k:k + 1], wcol_ref[:, k:k + 1], 0.0)
        high = weight.astype(BF16)
        whi[:, at] = high
        wlo[:, at] = (weight - high.astype(F32)).astype(BF16)
        return carry

    lax.fori_loop(0, 8, build_a, 0)

    pl.semaphore_wait(barrier, NZ * NP)

    swap = push(p_my, p_ot, q_s, q_r, partner)
    swap.start()
    swap.wait_recv()
    total = p_my[...].astype(F32) + p_ot[...].astype(F32)
    res = (tok_ref[...].astype(F32) + total).astype(BF16)
    resid[...] = res
    ntwo[...] = rms_scale(res.astype(F32), gain_ref[...]).astype(BF16)

    def cols(k):
        return pl.ds(pl.multiple_of(c * HALF + k * 128, 128), 128)

    xr = jnp.concatenate([ntwo[:, cols(k)] for k in range(8)], axis=0)

    def d_send(i, j):
        to, e = place(i, j)
        return push(outt.at[e], rcv.at[c, me], d_s.at[e], d_r.at[me], to)

    def dispatch(i, carry):
        zt = (z + i) % NZ
        rows = nn_dot(amat[pl.ds(pl.multiple_of(zt * 256, 256), 256), :], xr).astype(BF16)
        outt[pl.ds(zt * NP, NP)] = rows.reshape(NP, 16, 128)

        def go(j, carry2):
            d_send(i, j).start()
            return carry2

        lax.fori_loop(jnp.where(i == 0, 1, 0), NP, go, 0)
        return carry

    lax.fori_loop(0, NZ, dispatch, 0)
    rcv[c, me] = outt[me]

    def h_send(k):
        at = pl.ds(k * NP, NP)
        return push(rcv.at[c, at], rcv.at[c, at], h_s.at[k], h_r.at[k], partner)

    def land(i, carry):
        zs = (z + i) % NZ

        def take(j, carry2):
            _, s = place(i, j)
            push(rcv.at[c, s], rcv.at[c, s], d_r.at[s], d_r.at[s], partner).wait_recv()
            return carry2

        lax.fori_loop(jnp.where(i == 0, 1, 0), NP, take, 0)
        h_send(zs).start()
        return carry

    lax.fori_loop(0, NZ, land, 0)

    def unpack(side):
        xf[...] = rcv[side].astype(F32).reshape(2048, 128)
        for k in range(8):
            xm[:, pl.ds(pl.multiple_of(side * HALF + k * 128, 128), 128)] = xf[
                pl.ds(k, 256, stride=8), :
            ].astype(BF16)

    unpack(c)

    def forwarded(k, carry):
        at = pl.ds(k * NP, NP)
        push(rcv.at[1 - c, at], rcv.at[1 - c, at], h_r.at[k], h_r.at[k], partner).wait_recv()
        return carry

    lax.fori_loop(0, NZ, forwarded, 0)
    unpack(1 - c)

    for load in loads:
        load.wait()

    for lo, hi in ((0, 256), (256, 512), (512, DE)):
        gate = nn_dot(xm[...], wg[:, lo:hi])
        up = nn_dot(xm[...], wu[:, lo:hi])
        hid[:, lo:hi] = (gate * jax.nn.sigmoid(gate) * up).astype(BF16)

    def down(k, carry):
        for s in range(2):
            part2 = nn_dot(hid[...], wd[:, pl.ds(pl.multiple_of(s * HALF + k * 256, 256), 256)])
            pd[s, :, pl.ds(pl.multiple_of(k * 256, 256), 256)] = part2.astype(BF16)
        return carry

    lax.fori_loop(0, 4, down, 0)

    trade = push(pd.at[1 - c], pd_ot, k_s, k_r, partner)
    trade.start()
    trade.wait_recv()
    for k in range(8):
        at = slice(k * 128, (k + 1) * 128)
        xf[pl.ds(k, 256, stride=8), :] = pd[c, :, at].astype(F32) + pd_ot[:, at].astype(F32)
    back[...] = xf[...].astype(BF16).reshape(128, 16, 128)

    def b_send(i, j):
        to, s = place(i, j)
        return push(back.at[s], ret.at[me], b_s.at[s], b_r.at[me], to)

    over_peers(lambda i, j: b_send(i, j).start())
    ret[me] = back[me]

    def b_wait(i, j):
        _, s = place(i, j)
        push(ret.at[s], ret.at[s], b_r.at[s], b_r.at[s], partner).wait_recv()

    over_peers(b_wait)

    rows = ret[...].reshape(2048, 128)
    weighted = nn_dot(whi[...], rows) + nn_dot(wlo[...], rows)
    for k in range(8):
        mixed_ref[:, cols(k)] = (
            resid[:, cols(k)].astype(F32) + weighted[ROWS * k:ROWS * (k + 1)]
        ).astype(BF16)
    last = push(mixed_ref.at[:, half], mixed_ref.at[:, half], m_s, m_r, partner)
    last.start()
    push(mixed_ref.at[:, other], mixed_ref.at[:, other], m_s, m_r, partner).wait_recv()

    last.wait_send()
    swap.wait_send()
    trade.wait_send()

    def h_sent(k, carry):
        h_send(k).wait_send()
        return carry

    lax.fori_loop(0, NZ, h_sent, 0)

    def sent(i, j):
        d_send(i, j).wait_send()
        b_send(i, j).wait_send()

    over_peers(sent)


def experts(cell_out, tokens, ffn_gain, wof, crow, ccol, wcol, wg, wu, wd):
    dma = pltpu.SemaphoreType.DMA
    vm = pl.BlockSpec(memory_space=pltpu.VMEM)
    hbm = pl.BlockSpec(memory_space=pl.ANY)
    return pl.pallas_call(
        expert_kernel,
        name="experts",
        out_shape=jax.ShapeDtypeStruct((ROWS, D), BF16),
        in_specs=[vm] * 7 + [hbm] * 3,
        out_specs=vm,
        scratch_shapes=[
            pltpu.VMEM((ROWS, D), BF16),
            pltpu.VMEM((ROWS, D), BF16),
            pltpu.VMEM((ROWS, D), BF16),
            pltpu.VMEM((ROWS, D), BF16),
            pltpu.VMEM((2048, 256), BF16),
            pltpu.VMEM((256, 2048), BF16),
            pltpu.VMEM((256, 2048), BF16),
            pltpu.VMEM((128, 16, 128), BF16),
            pltpu.VMEM((2, 128, 16, 128), BF16),
            pltpu.VMEM((2048, 128), F32),
            pltpu.VMEM((256, D), BF16),
            pltpu.VMEM((D, DE), BF16),
            pltpu.VMEM((D, DE), BF16),
            pltpu.VMEM((DE, D), BF16),
            pltpu.VMEM((256, DE), BF16),
            pltpu.VMEM((2, 256, HALF), BF16),
            pltpu.VMEM((256, HALF), BF16),
            pltpu.VMEM((128, 16, 128), BF16),
            pltpu.VMEM((128, 16, 128), BF16),
            dma((3,)),
            dma, dma,
            dma((128,)), dma((128,)),
            dma((NZ,)), dma((NZ,)),
            dma, dma,
            dma((128,)), dma((128,)),
            dma, dma,
        ],
        compiler_params=pltpu.CompilerParams(
            collective_id=1, has_side_effects=True, vmem_limit_bytes=56 << 20
        ),
    )(cell_out, tokens, ffn_gain.reshape(1, D), wof, crow, ccol, wcol, wg, wu, wd)


def memory_cell(query, key_row, value_row, outgate, input_pre, forget_pre, head_gain,
                state_matrix, state_norm, state_max):
    seq_rows, head_count = input_pre.shape
    head_size = query.shape[1] // head_count
    query_heads = query.astype(F32).reshape(seq_rows, head_count, head_size)
    key_heads = key_row.astype(F32).reshape(seq_rows, head_count, head_size) * head_size ** (-0.5)
    value_heads = value_row.astype(F32).reshape(seq_rows, head_count, head_size)
    log_forget = jax.nn.log_sigmoid(forget_pre)
    new_max = jnp.maximum(log_forget + state_max, input_pre)
    keep_old = jnp.exp(log_forget + state_max - new_max)
    keep_new = jnp.exp(input_pre - new_max)
    new_matrix = (
        keep_old[:, :, None, None] * state_matrix
        + keep_new[:, :, None, None] * value_heads[:, :, :, None] * key_heads[:, :, None, :]
    )
    new_norm = keep_old[:, :, None] * state_norm + keep_new[:, :, None] * key_heads
    numerator = jnp.einsum("bhvd,bhd->bhv", new_matrix, query_heads)
    denominator = jnp.sum(new_norm * query_heads, axis=-1)
    cell_read = numerator / jnp.maximum(jnp.abs(denominator), jnp.exp(-new_max))[:, :, None]
    centered = cell_read - jnp.mean(cell_read, axis=-1, keepdims=True)
    variance = jnp.mean(centered * centered, axis=-1, keepdims=True)
    scaled_cell = (centered * lax.rsqrt(variance + 1e-06)).reshape(seq_rows, head_count * head_size)
    cell_out = (scaled_cell * head_gain * jax.nn.sigmoid(outgate.astype(F32))).astype(BF16)
    return (cell_out, new_matrix, new_norm, new_max)


def body(tokens, mix_gain, w_query, w_key, w_value, w_outgate, w_igate, w_fgate, igate_bias,
         fgate_bias, head_gain, w_out, state_matrix, state_norm, state_max, ffn_gain,
         w_expert_gate, w_expert_up, w_expert_down, routes, route_weights):
    z = lax.axis_index("ep_0")
    main = jnp.stack((w_query, w_key, w_value, w_outgate)).reshape(4, 16, NZ, 32)
    main = main.transpose(2, 1, 0, 3).reshape(NZ, 16, 128)
    gate_cols = jnp.tile(jnp.concatenate((w_igate, w_fgate), axis=1), (1, 16))
    lane = jnp.arange(128, dtype=jnp.int32)[None, :]
    gate_tile = jnp.where(lane // 8 == z, gate_cols, jnp.zeros_like(gate_cols))
    wp = jnp.concatenate((main, jnp.broadcast_to(gate_tile[None], (NZ, 16, 128))), axis=1)
    proj, gates, wof = gather(tokens, mix_gain, wp, w_out.T)
    parts = proj.reshape(NZ, ROWS, 4, 32).transpose(2, 1, 0, 3).reshape(4, ROWS, 256)
    input_pre = gates[:, 0:4] + igate_bias
    forget_pre = gates[:, 4:8] + fgate_bias
    cell_out, new_matrix, new_norm, new_max = memory_cell(
        parts[0], parts[1], parts[2], parts[3], input_pre, forget_pre, head_gain,
        state_matrix, state_norm, state_max,
    )
    flat = routes.reshape(-1)
    owner = jnp.arange(96, dtype=jnp.int32) // 3
    same = (flat[:, None] == flat[None, :]) & (owner[None, :] < owner[:, None])
    slot = jnp.sum(same.astype(jnp.int32), axis=1)
    code = ((flat * 2 + slot) * 8).reshape(ROWS, 3)
    fb = jnp.arange(8, dtype=jnp.int32)
    crow = (code.T[:, None, :] + fb[None, :, None]).reshape(3, 256)
    ccol = (code[None, :, :] + fb[:, None, None]).reshape(256, 3)
    wcol = jnp.broadcast_to(route_weights[None], (8, ROWS, 3)).reshape(256, 3)
    mixed = experts(cell_out, tokens, ffn_gain, wof, crow, ccol, wcol,
                    w_expert_gate, w_expert_up, w_expert_down)
    return (mixed, new_matrix, new_norm, new_max)


def solution(mesh):
    torus = Mesh(mesh.devices.reshape(NZ, NY, NX, mesh.shape["tp"]), (*EP, "tp"))
    placed = (
        P(EP, None), P(), P(EP, "tp"), P(EP, "tp"), P(EP, "tp"), P(EP, "tp"), P(EP, "tp"),
        P(EP, "tp"), P("tp"), P("tp"), P("tp"), P("tp", EP), P(EP, "tp", None, None),
        P(EP, "tp", None), P(EP, "tp"), P(), P(EP, None, "tp"), P(EP, None, "tp"),
        P(EP, "tp", None), P(EP, None), P(EP, None),
    )
    return jax.shard_map(
        body,
        mesh=torus,
        in_specs=placed,
        out_specs=(P(EP, None), P(EP, "tp", None, None), P(EP, "tp", None), P(EP, "tp")),
        check_vma=False,
    )
```

time: 302 us -> 141 us (0.47)
  waiting for transfers between devices: 144 us -> 0 us
  Pallas kernels: 0 us -> 103 us
  blocking collectives: 79.1 us -> 0 us
  matrix products: 26.3 us -> 3.51 us
  between operations: 14.3 us -> 0.9 us
  starting transfers between devices: 7.4 us -> 0 us
    all_gather x2 -> x0, waiting for transfers between devices: 115 us -> none  [the longest x1 95.9 us: sent_together(): filled, at, done = (lax.all_gather(both, axis, axis=dim, tiled=True), 0, [])]
    pallas_call x0 -> x2, Pallas kernels: none -> 103 us  [the longest x1 68.1 us: experts(): pl.pallas_call(expert_kernel, name='experts', out_shape=jax.ShapeDtypeStr...]
    all_to_all x3 -> x0, blocking collectives: 58.3 us -> none  [the longest x1 40 us: body(): lax.all_to_all(outgoing, EP, split_axis=0, concat_axis=0, tiled=True)]
    all_to_all x1 -> x0, waiting for transfers between devices: 29 us -> none  [body(): lax.all_to_all(finished, EP, split_axis=0, concat_axis=0, tiled=True)]
    dot_general x10 -> x0, matrix products: 25.1 us -> none  [the longest x5 7.95 us: body(): jnp.dot(normed, shard_piece, preferred_element_type=jnp.float32)]
    all_gather x2 -> x0, blocking collectives: 20.8 us -> none  [gathered_by_axis(): nearer = lax.all_gather(value, axes[-1], axis=dim, tiled=True)]
    unnamed x25 -> x23, local copies, waits for them, and re-layouts: 5.51 us -> 13.9 us
    all_to_all x1 -> x0, starting transfers between devices: 7.32 us -> none  [body(): lax.all_to_all(finished, EP, split_axis=0, concat_axis=0, tiled=True)]
  transfers between devices with their start and end apart: 3 -> 0, of which waited for: 3 -> 0; matrix products, arithmetic and copies ran while one was open for 6% -> 0% of each run, Pallas kernels for 0% -> 0%
where the time goes in v1:
time: 141 us; the launch traced here: 140 us
  Pallas kernels  103 us (73%)
  local copies, waits for them, and re-layouts  19.5 us (14%)
  other arithmetic  13 us (9%)
  matrix products  3.51 us (2%)
    pallas_call x1, Pallas kernels, experts(): pl.pallas_call(expert_kernel, name='experts', out_shape=jax.ShapeDtypeStr...  68.1 us
    pallas_call x1, Pallas kernels, gather(): pl.pallas_call(gather_kernel, name='gather', out_shape=(jax.ShapeDtypeStr...  35 us
    unnamed x23, local copies, waits for them, and re-layouts  13.9 us
    add x1, other arithmetic, memory_cell(): keep_old[:, :, None, None] * state_matrix  5.88 us
    dot_general x1, matrix products, memory_cell(): numerator = jnp.einsum('bhvd,bhd->bhv', new_matrix, query_heads)  3.51 us
    another operation x8, local copies, waits for them, and re-layouts, body(): jnp.stack((w_query, w_key, w_value, w_outgate)).reshape(4, 16, NZ, 32)  3.36 us

profile of v1, /device:TPU:1, one launch (start us, length us, event | category | flops | bytes accessed | tf_op | source)
XLA Modules:
  0.0 140.0 jit_solution(2382870934624783322)
XLA Ops:
  0.6 0.8 stack.15
  1.4 0.1 copy.70
  1.5 0.8 stack.16
  2.3 0.1 copy.71
  2.3 0.8 stack.17
  3.1 0.1 copy.72
  3.2 0.8 stack.18
  4.0 0.1 copy.73
  4.0 0.4 maximum_bitcast_fusion
  4.4 0.1 reshape.208
  4.6 0.7 pad_maximum_fusion.1
  5.3 0.1 bitcast_select_fusion
  5.4 0.1 copy.74
  5.5 0.0 copy-start.1
  5.5 0.9 copy-done.1
  6.4 0.0 copy-start.2
  6.4 0.7 copy-done.2
  7.1 0.0 copy-start.3
  7.1 0.7 copy-done.3
  7.8 35.0 %gather.1 = (bf16[8,32,128]{2,1,0:T(8,128)(2,1)S(1)}, f32[32,128]{1,0:T(8,128)S(1)}, bf16[8,16,16,256]{3,2,1,0:T(8,128)(2,1)S(1)}) custom-call(bf16[32,2048]{1,0:T(8,128)(2,1)S(1)} %copy-done.1, f32[1,2048]{1,0:T(1,128)S(1)} %bitcast.28, bf16[8,32,128]{2,1,0:T(8,128)(2,1)S(1)} %pad_maximum_fusion.wp_ref, bf16[16,256]{1,0:T(8,128)(2,1)S(1)} %bitcast.29), custom_call_target="tpu_custom_call" | custom-call | tf_op jit(solution)/shard_map/gather/pallas_call | solution.py:228
  42.8 0.0 copy-start
  42.8 1.0 copy-done
  43.8 0.8 copy.75
  44.5 0.8 broadcast_multiply_fusion.3
  45.3 0.8 subtract_exponential_fusion.1
  46.1 0.2 reshape.209
  46.2 0.2 copy.87
  46.5 0.1 reshape.210
  46.6 0.1 reshape.214
  46.7 0.1 reshape.215
  46.8 1.6 %multiply_reduce_fusion.1 = (f32[32,4]{1,0:T(8,128)S(1)}, f32[32,4,64]{2,1,0:T(4,128)}, f32[32,4,64]{2,1,0:T(4,128)S(1)}, f32[32,4,64]{2,1,0:T(4,128)S(1)}) fusion(bf16[32,4,64]{2,1,0:T(4,128)(2,1)S(1)} %reshape.210, f32[32,4,64]{2,1,0:T(4,128)S(1)} %reshape.215, f32[32,4]{1,0:T(8,128)S(1)} %get-tuple-element.30, f32[32,4,64]{2,1,0:T(4,128)} %param.34, ...), kind=kLoop, calls=%fused_computation.9 | loop fusion | flops 65408 | bytes 215040 | tf_op jit(solution)/shard_map/reduce_sum | solution.py:513
  48.4 5.9 %multiply_add_fusion = f32[32,4,64,64]{3,2,1,0:T(8,128)} fusion(f32[32,4,64,64]{3,2,1,0:T(8,128)} %param.33, f32[32,4,64]{2,1,0:T(4,128)S(1)} %get-tuple-element.36, f32[32,4,64]{2,1,0:T(4,128)S(1)} %get-tuple-element.37, f32[32,4]{1,0:T(8,128)S(1)} %subtract_exponential_fusion.1), kind=kLoop, calls=%fused_computation | loop fusion | flops 1572864 | bytes 4260352 | tf_op jit(solution)/shard_map/add | solution.py:508
  54.3 0.0 copy-start.7
  54.3 0.0 copy-start.5
  54.3 0.0 copy-start.4
  54.3 0.1 reshape.221
  54.4 3.5 %fusion.7 = f32[32,4,1,64]{3,2,1,0:T(1,128)S(1)} fusion(f32[32,4,64,64]{3,2,1,0:T(8,128)} %multiply_add_fusion, bf16[32,4,64,1]{2,3,1,0:T(2,128)(2,1)S(1)} %reshape.221), kind=kOutput, calls=%fused_computation.43 | convolution fusion | flops 1048576 | bytes 2146304 | tf_op jit(solution)/shard_map/bhvd,bhd->bhv/dot_general | solution.py:512
  57.9 0.2 fusion.4
  58.1 0.2 multiply_reduce_fusion
  58.3 0.1 subtract_multiply_fusion
  58.5 0.1 reshape.211
  58.6 0.1 reshape.217
  58.7 0.0 copy-done.7
  58.7 0.6 multiply_convert_fusion.cell_ref
  59.3 0.0 copy-done.5
  59.3 0.1 copy.77
  59.4 0.1 eq.28
  59.5 0.2 convert_reduce_fusion
  59.7 0.1 reduce_sum.42
  59.8 0.1 copy.78
  59.9 0.1 copy.79
  60.0 0.1 add.125
  60.1 0.8 bitcast_add_fusion.ccol_ref
  60.9 0.1 add.123
  60.9 0.6 broadcast_add_fusion.crow_ref
  61.5 0.0 copy-done.4
  61.5 2.8 %copy.81.wg_hbm = bf16[1,2048,704]{2,1,0:T(8,128)(2,1)} copy(bf16[1,2048,704]{1,2,0:T(8,128)(2,1)S(1)} %copy-done.4) | data formatting | bytes 5767168 | tf_op args[16]
  64.3 4.6 %copy.82.wu_hbm = bf16[1,2048,704]{2,1,0:T(8,128)(2,1)} copy(bf16[1,2048,704]{1,2,0:T(8,128)(2,1)} %param.38) | data formatting | bytes 5767168 | tf_op args[17]
  69.0 0.0 copy-done.6
  69.0 0.1 copy.80
  69.0 0.7 broadcast_in_dim.17
  69.7 68.1 %experts.1 = bf16[32,2048]{1,0:T(8,128)(2,1)} custom-call(bf16[32,256]{1,0:T(8,128)(2,1)} %multiply_convert_fusion.cell_ref, bf16[32,2048]{1,0:T(8,128)(2,1)} %tok_ref.3, f32[1,2048]{1,0:T(1,128)} %bitcast.35, bf16[8,16,16,256]{3,2,1,0:T(8,128)(2,1)} %copy-done, s32[3,256]{1,0:T(4,128)} %broadcast_add_fusion.crow_ref, s32[256,3]{1,0:T(8,128)} %bitcast_add_fusion.ccol_ref, ...), custom_call_target="tpu_custom_call" | custom-call | tf_op jit(solution)/shard_map/experts/pallas_call | solution.py:456
  137.8 0.7 copy.83
  138.5 1.6 %copy.89 = bf16[32,2048]{1,0:T(8,128)(2,1)} copy(bf16[32,2048]{1,0:T(8,128)(2,1)} %experts.1) | data formatting | bytes 262144
  (13 shorter events, 0.2 us)
Async XLA Ops:
  5.5 0.9 copy-start.1
  6.4 0.7 copy-start.2
  7.1 0.7 copy-start.3
  42.8 1.0 copy-start
  54.3 4.4 %copy-start.7 = (f32[256]{0:T(256)S(1)}, f32[256]{0:T(256)}, u32[]{:S(2)}) copy-start(f32[256]{0:T(256)} %param.31) | copy-start | bytes 3076
  54.3 5.1 %copy-start.5 = (s32[32,3]{0,1:T(4,128)S(1)}, s32[32,3]{0,1:T(4,128)}, u32[]{:S(2)}) copy-start(s32[32,3]{0,1:T(4,128)} %param.40) | copy-start | bytes 1156
  54.3 7.3 %copy-start.4 = (bf16[1,2048,704]{1,2,0:T(8,128)(2,1)S(1)}, bf16[1,2048,704]{1,2,0:T(8,128)(2,1)}, u32[]{:S(2)}) copy-start(bf16[1,2048,704]{1,2,0:T(8,128)(2,1)} %param.37) | copy-start | bytes 8650756
  64.3 4.6 %copy-start.6 = (f32[32,3]{0,1:T(4,128)S(1)}, f32[32,3]{0,1:T(4,128)}, u32[]{:S(2)}) copy-start(f32[32,3]{0,1:T(4,128)} %param.41) | copy-start | bytes 1156

commit v2 on v0

v2 whole, which is shorter than its diff:
```python
import jax
import jax.numpy as jnp
from jax import lax
from jax.experimental import pallas as pl
from jax.experimental.pallas import tpu as pltpu
from jax.sharding import Mesh
from jax.sharding import PartitionSpec as P

EP = ("ep_0", "ep_1", "ep_2")
NZ, NY, NX = 8, 4, 4
NP = NY * NX
D, HALF = 2048, 1024
DE = 704
ROWS = 32
MESH = pl.DeviceIdType.MESH
F32, BF16 = jnp.float32, jnp.bfloat16


def whereami():
    return (
        lax.axis_index("ep_0"),
        lax.axis_index("ep_1"),
        lax.axis_index("ep_2"),
        lax.axis_index("tp"),
    )


def push(src, dst, send_sem, recv_sem, to):
    return pltpu.make_async_remote_copy(
        src_ref=src,
        dst_ref=dst,
        send_sem=send_sem,
        recv_sem=recv_sem,
        device_id=to,
        device_id_type=MESH,
    )


def nt_dot(a, b):
    return lax.dot_general(a, b, (((1,), (1,)), ((), ())), preferred_element_type=F32)


def nn_dot(a, b):
    return jnp.dot(a, b, preferred_element_type=F32)


def rms_scale(values, gain):
    return values * lax.rsqrt(jnp.mean(values * values, axis=-1, keepdims=True) + 1e-06) * gain


ZOFF = (4, 3, 5, 2, 6, 1, 7)


def fused_kernel(
    tok_h, mg_h, wq_h, wk_h, wv_h, wg_h, ig_h, fg_h, ib_h, fb_h, hg_h, wo_h, sm_h, sn_h, fgain_h,
    rt_h, rw_h, st_h, eg_h, eu_h, ed_h,
    mixed_ref, nmat_h, nnorm_ref, nmax_ref,
    tok, mg, wq, wk, wv, wg, ig, fg, ib, fb, hg, wo, sm, sn, fgain, rt, rw, st, eg, eu, ed,
    nall, wst, gst, gtile, gsum, wfull, gt, woz, wof, res, proj, tbuf, b8,
    qrow, kcol, keep, scal, vt, cell,
    p_my, p_ot, resid, ntwo, amat, wmat, outt, rcv, xf, xm, hid, pd, pd_ot, own, yf, back, ret,
    ld, out_sem, n_r, f_s, f_r, one_s, one_r, d_r, h_s, h_r, k_r, b_r,
):
    z, y, x, c = whereami()
    yx = y * NX + x
    me = z * NP + yx
    partner = (z, y, x, 1 - c)
    half = pl.ds(pl.multiple_of(c * HALF, HALF), HALF)
    other = pl.ds(pl.multiple_of((1 - c) * HALF, HALF), HALF)

    ins = (tok_h, mg_h, wq_h, wk_h, wv_h, wg_h, ig_h, fg_h, ib_h, fb_h, hg_h, wo_h, sm_h, sn_h,
           fgain_h, rt_h, rw_h, st_h, eg_h.at[0], eu_h.at[0], ed_h.at[0])
    dsts = (tok, mg, wq, wk, wv, wg, ig, fg, ib, fb, hg, wo, sm, sn, fgain, rt, rw, st, eg, eu, ed)
    loads = [pltpu.make_async_copy(a, b, ld.at[k]) for k, (a, b) in enumerate(zip(ins, dsts))]
    for load in loads:
        load.start()

    def zpeer(d):
        return (z + d) % NZ

    def ppeer(d):
        yt, xt = (y + d // NX) % NY, (x + d % NX) % NX
        return yt, xt, yt * NX + xt

    def loop(lo, hi, body):
        def step(k, carry):
            body(k)
            return carry

        lax.fori_loop(lo, hi, step, 0)

    def place(off, j):
        zt = zpeer(off)
        yt, xt, yxt = ppeer(j)
        return (zt, yt, xt, c), zt * NP + yxt

    barrier = pltpu.get_barrier_semaphore()

    def greet_plane(off, lo):
        def greet(j):
            to, _ = place(off, j)
            pl.semaphore_signal(barrier, 1, device_id=to, device_id_type=MESH)

        loop(lo, NP, greet)

    loop(1, NZ, lambda i: greet_plane(i, 0))
    greet_plane(0, 1)
    pl.semaphore_signal(barrier, 1, device_id=partner, device_id_type=MESH)

    for load in loads[:18]:
        load.wait()

    nall[z] = rms_scale(tok[...].astype(F32), mg[...]).astype(BF16)

    tbuf[...] = jnp.zeros((128, 128), F32)
    b8[...] = jnp.zeros((8, 128), F32)
    b8[0:4, 0:16] = ig[...].astype(F32)
    b8[4:8, 0:16] = fg[...].astype(F32)
    tbuf[pl.ds(pl.multiple_of(z * 8, 8), 8), :] = b8[...]
    gtile[...] = tbuf[...].T[0:16, :].astype(BF16)

    pl.semaphore_wait(barrier, NZ * NP)

    wsrc = (wq, wk, wv, wg)

    def w_send(t):
        return push(
            wsrc[t // 2].at[:, (t % 2) * 128:(t % 2 + 1) * 128], wst.at[z],
            one_s.at[0], one_r.at[0], (t, y, x, c),
        )

    for t in range(NZ):
        @pl.when(z != t)
        def _(t=t):
            w_send(t).start()

        @pl.when(z == t)
        def _(t=t):
            wst[t] = wsrc[t // 2][:, (t % 2) * 128:(t % 2 + 1) * 128]

    def gz_send(d):
        return push(gtile, gst.at[z], one_s.at[1], one_r.at[1], (zpeer(d), y, x, c))

    def o_send(d):
        return push(wo, woz.at[z], one_s.at[2], one_r.at[2], (zpeer(d), y, x, c))

    def n_send(d):
        return push(nall.at[z, :, half], nall.at[z, :, half], one_s.at[3], n_r.at[z],
                    (zpeer(d), y, x, c))

    for d in ZOFF:
        gz_send(d).start()
    for d in ZOFF:
        n_send(d).start()
    for d in ZOFF:
        o_send(d).start()
    gst[z] = gtile[...]
    woz[z] = wo[...]

    def arrived(view, recv_sem):
        push(view, view, recv_sem, recv_sem, partner).wait_recv()

    def left(view, send_sem):
        push(view, view, send_sem, send_sem, partner).wait_send()

    arrived(wst.at[0:7], one_r.at[0])
    arrived(gst.at[0:7], one_r.at[1])
    total = gst[0].astype(F32)
    for k in range(1, NZ):
        total = total + gst[k].astype(F32)
    gsum[...] = total.astype(BF16)
    gt[yx] = gsum[...]
    for k in range(NZ):
        wfull[k, yx] = wst[k]

    def x_send(d):
        yt, xt, _ = ppeer(d)
        return push(wst, wfull.at[:, yx], one_s.at[4], one_r.at[4], (z, yt, xt, c))

    def g_send(d):
        yt, xt, _ = ppeer(d)
        return push(gsum, gt.at[yx], one_s.at[5], one_r.at[5], (z, yt, xt, c))

    def v_send(d):
        yt, xt, _ = ppeer(d)
        return push(woz, wof.at[:, yx], one_s.at[6], one_r.at[6], (z, yt, xt, c))

    loop(1, NP, lambda d: x_send(d).start())
    loop(1, NP, lambda d: g_send(d).start())

    tbuf[...] = jnp.zeros((128, 128), F32)
    tbuf[0:3, 0:32] = rt[...].astype(F32)
    tbuf[8:11, 0:32] = rw[...]
    tbuf[16:20, 0:32] = sm[...]
    side = tbuf[...].T
    smax = side[0:ROWS, 16:20]
    earlier = lax.broadcasted_iota(jnp.int32, (ROWS, ROWS), 1) < lax.broadcasted_iota(
        jnp.int32, (ROWS, ROWS), 0
    )
    lane256 = lax.broadcasted_iota(jnp.int32, (256, 128), 1)
    fbs = (lax.broadcasted_iota(jnp.int32, (256, 1), 0) // ROWS).astype(F32)
    code_cols, weight_cols = [], []
    table = jnp.zeros((256, 128), F32)
    for k in range(3):
        mine = side[0:ROWS, k:k + 1]
        count = jnp.zeros((ROWS, 1), F32)
        for k2 in range(3):
            theirs = tbuf[k2:k2 + 1, 0:ROWS]
            same = (mine == theirs) & earlier
            count = count + jnp.sum(jnp.where(same, 1.0, 0.0), axis=1, keepdims=True)
        code = (mine * 2.0 + count) * 8.0
        code_cols.append(jnp.concatenate([code] * 8, axis=0) + fbs)
        weight_cols.append(jnp.concatenate([side[0:ROWS, 8 + k:9 + k]] * 8, axis=0))
        table = table + jnp.where(lane256 == k, code_cols[k], 0.0)
    rows_t = table.T

    for i in range(8):
        at = slice(i * 256, (i + 1) * 256)
        row = (lax.broadcasted_iota(jnp.int32, (256, 256), 0) + i * 256).astype(F32)
        hit = (row == rows_t[0:1, :]) | (row == rows_t[1:2, :]) | (row == rows_t[2:3, :])
        amat[at, :] = jnp.where(hit, 1.0, 0.0).astype(BF16)
        col = (lax.broadcasted_iota(jnp.int32, (256, 256), 1) + i * 256).astype(F32)
        weight = jnp.zeros((256, 256), F32)
        for k in range(3):
            weight = weight + jnp.where(col == code_cols[k], weight_cols[k], 0.0)
        high = weight.astype(BF16)
        wmat[0:256, at] = high
        wmat[256:512, at] = (weight - high.astype(F32)).astype(BF16)

    arrived(woz.at[0:7], one_r.at[2])
    for k in range(NZ):
        wof[k, yx] = woz[k]
    loop(1, NP, lambda d: v_send(d).start())

    def f_send(zs):
        return push(nall.at[zs, :, half], nall.at[zs, :, half], f_s, f_r.at[zs], partner)

    for d in (1, 7, 2, 6, 3, 5, 4):
        zs = zpeer(d)
        arrived(nall.at[zs, :, half], n_r.at[zs])
        f_send(zs).start()

    arrived(gt.at[0:15], one_r.at[5])
    mine = nall[z]
    stacked = jnp.concatenate([mine[:, 256 * k:256 * (k + 1)] for k in range(NZ)], axis=0)
    gp = nn_dot(stacked, gt[...].reshape(256, 128))
    group = lax.broadcasted_iota(jnp.int32, (ROWS, 128), 1) // 8
    gates = jnp.zeros((ROWS, 128), F32)
    for k in range(NZ):
        gates = gates + jnp.where(group == k, gp[ROWS * k:ROWS * (k + 1)], 0.0)
    for shift in (64, 32, 16, 8):
        gates = gates + pltpu.roll(gates, shift, 1)
    input_pre = gates[:, 0:4] + ib[...]
    forget_pre = gates[:, 4:8] + fb[...]
    log_forget = jnp.minimum(forget_pre, 0.0) - jnp.log1p(jnp.exp(-jnp.abs(forget_pre)))
    new_max = jnp.maximum(log_forget + smax, input_pre)
    keep_old = jnp.exp(log_forget + smax - new_max)
    keep_new = jnp.exp(input_pre - new_max)
    floor = jnp.exp(-new_max)
    tbuf[...] = jnp.zeros((128, 128), F32)
    tbuf[0:ROWS, 0:4] = new_max
    nmax_ref[...] = tbuf[...].T[0:4, 0:ROWS]

    for d in (1, 7, 2, 6, 3, 5, 4):
        zs = zpeer(d)
        arrived(nall.at[zs, :, other], f_r.at[zs])
    arrived(wfull.at[:, 0:15], one_r.at[4])

    every = nn_dot(nall[...].reshape(NZ * ROWS, D), wfull[...].reshape(D, 128))
    res[...] = every.astype(BF16).reshape(NZ, ROWS, 128)

    def p_send(d):
        zt = zpeer(d)
        return push(res.at[zt], proj.at[z], one_s.at[7], one_r.at[7], (zt, y, x, c))

    for d in ZOFF:
        p_send(d).start()
    proj[z] = res[z]
    arrived(proj.at[0:7], one_r.at[7])

    lane = lax.broadcasted_iota(jnp.int32, (ROWS, 128), 1)
    low = lane < 64

    def spread(pair):
        return jnp.where(low, pair[0], pair[1])

    def pair_sum(v):
        return (
            jnp.sum(jnp.where(low, v, 0.0), axis=1, keepdims=True),
            jnp.sum(jnp.where(low, 0.0, v), axis=1, keepdims=True),
        )

    eye = jnp.where(
        lax.broadcasted_iota(jnp.int32, (128, 128), 0) == lax.broadcasted_iota(jnp.int32, (128, 128), 1),
        1.0, 0.0,
    ).astype(BF16)
    for p in range(2):
        q = proj[p].astype(F32)
        for h in range(2):
            qrow[2 * p + h] = q[:, 64 * h:64 * (h + 1)]
            kcol[2 * p + h] = proj[2 + p][:, 64 * h:64 * (h + 1)]
        vt[p] = nt_dot(eye, proj[4 + p]).astype(BF16)
        for h in range(2):
            n = 2 * p + h
            keep[n] = jnp.broadcast_to(keep_old[:, n:n + 1], (ROWS, 64))
            scal[n] = jnp.broadcast_to(keep_new[:, n:n + 1] * 0.125, (ROWS, 64))

    lane64 = lax.broadcasted_iota(jnp.int32, (64, 128), 1)

    def read_one(b, acc):
        done = []
        for h in range(4):
            prod = st[b, h] * qrow[h, pl.ds(b, 1), :]
            done.append(jnp.where(lane64 == b, jnp.sum(prod, axis=1, keepdims=True), acc[h]))
        return tuple(done)

    acc = lax.fori_loop(0, ROWS, read_one, tuple(jnp.zeros((64, 128), F32) for _ in range(4)))

    for p in range(2):
        q, kk, vv = proj[p].astype(F32), proj[2 + p].astype(F32) * 0.125, proj[4 + p].astype(F32)
        gate = proj[6 + p].astype(F32)
        h0, h1 = 2 * p, 2 * p + 1

        def two(v):
            return v[:, h0:h0 + 1], v[:, h1:h1 + 1]

        ko, kn = two(keep_old), two(keep_new)
        tbuf[0:64, :] = acc[h0]
        tbuf[64:128, :] = acc[h1]
        num0 = tbuf[...].T[0:ROWS, :]
        norm_in = jnp.concatenate([sn[:, h0, :], sn[:, h1, :]], axis=1)
        norm_new = spread(ko) * norm_in + spread(kn) * kk
        nnorm_ref[:, h0, :] = norm_new[:, 0:64]
        nnorm_ref[:, h1, :] = norm_new[:, 64:128]
        den = pair_sum(norm_new * q)
        kq = pair_sum(kk * q)
        fl = two(floor)
        bottom = tuple(jnp.maximum(jnp.abs(den[i]), fl[i]) for i in range(2))
        read = (spread(ko) * num0 + spread(kn) * vv * spread(kq)) / spread(bottom)
        mean = tuple(v * (1.0 / 64) for v in pair_sum(read))
        centered = read - spread(mean)
        var = tuple(v * (1.0 / 64) for v in pair_sum(centered * centered))
        scaled = centered * lax.rsqrt(spread(var) + 1e-06)
        at = slice(p * 128, (p + 1) * 128)
        cell[:, at] = (scaled * hg[:, at] * jax.nn.sigmoid(gate)).astype(BF16)

    arrived(wof.at[:, 0:15], one_r.at[6])
    p_my[...] = nt_dot(cell[...], wof[...].reshape(D, 256)).astype(BF16)
    swap = push(p_my, p_ot, one_s.at[8], one_r.at[8], partner)
    swap.start()
    swap.wait_recv()
    both = p_my[...].astype(F32) + p_ot[...].astype(F32)
    rsd = (tok[...].astype(F32) + both).astype(BF16)
    resid[...] = rsd
    ntwo[...] = rms_scale(rsd.astype(F32), fgain[...]).astype(BF16)

    def cols(s, k):
        return pl.ds(pl.multiple_of(s * HALF + k * 128, 128), 128)

    xr = jnp.concatenate([ntwo[:, cols(c, k)] for k in range(8)], axis=0)

    def d_send(off, j):
        to, e = place(off, j)
        return push(outt.at[e], rcv.at[c, me], one_s.at[9], d_r.at[z], to)

    def plane256(zt):
        return pl.ds(pl.multiple_of(zt * 256, 256), 256)

    def plane16(zt):
        return pl.ds(zt * NP, NP)

    for off in (*ZOFF, 0):
        zt = zpeer(off)
        rows = nn_dot(amat[plane256(zt), :], xr).astype(BF16)
        outt[plane16(zt)] = rows.reshape(NP, 16, 128)
        loop(1 if off == 0 else 0, NP, lambda j, off=off: d_send(off, j).start())
    rcv[c, me] = outt[me]

    def write_one(b):
        for h in range(4):
            vth = vt[h // 2, 64 * (h % 2):64 * (h % 2 + 1), :]
            pick = jnp.where(
                lax.broadcasted_iota(jnp.int32, (64, ROWS), 1) == b, vth.astype(F32), 0.0
            ).astype(BF16)
            outer = nn_dot(pick, kcol[h])
            st[b, h] = keep[h, pl.ds(b, 1), :] * st[b, h] + scal[h, pl.ds(b, 1), :] * outer

    loop(0, ROWS, write_one)
    save = pltpu.make_async_copy(st, nmat_h, out_sem)
    save.start()

    def h_view(s, zs):
        return rcv.at[s, plane16(zs)]

    def h_send(zs):
        return push(h_view(c, zs), h_view(c, zs), h_s, h_r.at[zs], partner)

    def unpack(s, zs):
        xf[...] = rcv[s, plane16(zs)].astype(F32).reshape(256, 128)
        at = pl.ds(pl.multiple_of(zs * ROWS, ROWS), ROWS)
        for k in range(8):
            xm[at, cols(s, k)] = xf[pl.ds(k, ROWS, stride=8), :].astype(BF16)

    for off in (*ZOFF, 0):
        zs = (z + NZ - off) % NZ
        if off:
            arrived(rcv.at[c, plane16(zs)], d_r.at[zs])
        else:
            arrived(rcv.at[c, 0:15], d_r.at[zs])
        h_send(zs).start()
        unpack(c, zs)
    for off in (*ZOFF, 0):
        zs = (z + NZ - off) % NZ
        arrived(h_view(1 - c, zs), h_r.at[zs])
        unpack(1 - c, zs)

    for load in loads[18:]:
        load.wait()

    for lo, hi in ((0, 256), (256, 512), (512, DE)):
        gate = nt_dot(xm[...], eg[lo:hi, :])
        up = nt_dot(xm[...], eu[lo:hi, :])
        hid[:, lo:hi] = (gate * jax.nn.sigmoid(gate) * up).astype(BF16)

    def down(s, k):
        return nn_dot(hid[...], ed[:, pl.ds(pl.multiple_of(s * HALF + k * 256, 256), 256)]).astype(BF16)

    def k_send(k):
        return push(pd.at[k], pd_ot.at[k], one_s.at[10], k_r.at[k], partner)

    for k in range(4):
        pd[k] = down(1 - c, k)
        k_send(k).start()
    for k in range(4):
        own[k] = down(c, k)
    for k in range(4):
        arrived(pd_ot.at[k], k_r.at[k])
        both = own[k].astype(F32) + pd_ot[k].astype(F32)
        for h in range(2):
            yf[pl.ds(2 * k + h, 256, stride=8), :] = both[:, 128 * h:128 * (h + 1)]

    def b_send(off, j):
        to, s = place(off, j)
        return push(back.at[s], ret.at[me], one_s.at[11], b_r.at[z], to)

    for off in (*ZOFF, 0):
        zt = zpeer(off)
        back[plane16(zt)] = yf[plane256(zt), :].astype(BF16).reshape(NP, 16, 128)
        loop(1 if off == 0 else 0, NP, lambda j, off=off: b_send(off, j).start())
    ret[me] = back[me]

    weighted = jnp.zeros((512, 128), F32)
    for off in (*ZOFF, 0):
        zs = (z + NZ - off) % NZ
        if off:
            arrived(ret.at[plane16(zs)], b_r.at[zs])
        else:
            arrived(ret.at[0:15], b_r.at[zs])
        weighted = weighted + nn_dot(wmat[:, plane256(zs)], ret[plane16(zs)].reshape(256, 128))
    for k in range(8):
        mixed_ref[:, cols(c, k)] = (
            resid[:, cols(c, k)].astype(F32)
            + (weighted[ROWS * k:ROWS * (k + 1)] + weighted[256 + ROWS * k:256 + ROWS * (k + 1)])
        ).astype(BF16)
    last = push(mixed_ref.at[:, half], mixed_ref.at[:, half], one_s.at[12], one_r.at[12], partner)
    last.start()

    left(wst.at[0:7], one_s.at[0])
    left(gst.at[0:7], one_s.at[1])
    left(woz.at[0:7], one_s.at[2])
    left(nall.at[0:7, :, half], one_s.at[3])
    left(wfull.at[:, 0:15], one_s.at[4])
    left(gt.at[0:15], one_s.at[5])
    left(wof.at[:, 0:15], one_s.at[6])
    left(res.at[0:7], one_s.at[7])
    left(p_my, one_s.at[8])
    left(outt.at[0:127], one_s.at[9])
    left(pd, one_s.at[10])
    left(back.at[0:127], one_s.at[11])
    left(nall.at[0:7, :, half], f_s)
    left(outt, h_s)
    save.wait()
    arrived(mixed_ref.at[:, other], one_r.at[12])
    last.wait_send()


def fused(*args):
    dma = pltpu.SemaphoreType.DMA
    vm = pl.BlockSpec(memory_space=pltpu.VMEM)
    hbm = pl.BlockSpec(memory_space=pl.ANY)

    def buf(shape, kind=BF16):
        return pltpu.VMEM(shape, kind)

    staged = [buf(a.shape if a.ndim < 3 or a.shape[0] != 1 else a.shape[1:], a.dtype) for a in args]
    return pl.pallas_call(
        fused_kernel,
        name="layer",
        out_shape=(
            jax.ShapeDtypeStruct((ROWS, D), BF16),
            jax.ShapeDtypeStruct((ROWS, 4, 64, 64), F32),
            jax.ShapeDtypeStruct((ROWS, 4, 64), F32),
            jax.ShapeDtypeStruct((4, ROWS), F32),
        ),
        in_specs=[hbm] * len(args),
        out_specs=(vm, hbm, vm, vm),
        scratch_shapes=[
            *staged,
            buf((NZ, ROWS, D)),
            buf((NZ, 16, 128)),
            buf((NZ, 16, 128)),
            buf((16, 128)),
            buf((16, 128)),
            buf((NZ, NP, 16, 128)),
            buf((NP, 16, 128)),
            buf((NZ, 16, 256)),
            buf((NZ, NP, 16, 256)),
            buf((NZ, ROWS, 128)),
            buf((NZ, ROWS, 128)),
            buf((128, 128), F32),
            buf((8, 128), F32),
            buf((4, ROWS, 64), F32),
            buf((4, ROWS, 64)),
            buf((4, ROWS, 64), F32),
            buf((4, ROWS, 64), F32),
            buf((2, 128, ROWS)),
            buf((ROWS, 256)),
            buf((ROWS, D)),
            buf((ROWS, D)),
            buf((ROWS, D)),
            buf((ROWS, D)),
            buf((2048, 256)),
            buf((512, 2048)),
            buf((128, 16, 128)),
            buf((2, 128, 16, 128)),
            buf((256, 128), F32),
            buf((256, D)),
            buf((256, DE)),
            buf((4, 256, 256)),
            buf((4, 256, 256)),
            buf((4, 256, 256)),
            buf((2048, 128), F32),
            buf((128, 16, 128)),
            buf((128, 16, 128)),
            dma((len(args),)),
            dma,
            dma((NZ,)),
            dma,
            dma((NZ,)),
            dma((13,)),
            dma((13,)),
            dma((NZ,)),
            dma,
            dma((NZ,)),
            dma((4,)),
            dma((NZ,)),
        ],
        compiler_params=pltpu.CompilerParams(
            collective_id=0, has_side_effects=True, vmem_limit_bytes=58 << 20
        ),
    )(*args)


def body(tokens, mix_gain, w_query, w_key, w_value, w_outgate, w_igate, w_fgate, igate_bias,
         fgate_bias, head_gain, w_out, state_matrix, state_norm, state_max, ffn_gain,
         w_expert_gate, w_expert_up, w_expert_down, routes, route_weights):
    mixed, new_matrix, new_norm, new_max = fused(
        tokens, mix_gain.reshape(1, D), w_query, w_key, w_value, w_outgate, w_igate.T, w_fgate.T,
        igate_bias.reshape(1, 4), fgate_bias.reshape(1, 4), head_gain.reshape(1, 256), w_out.T,
        state_max.T, state_norm, ffn_gain.reshape(1, D), routes.T, route_weights.T, state_matrix,
        w_expert_gate.swapaxes(1, 2), w_expert_up.swapaxes(1, 2), w_expert_down,
    )
    return (mixed, new_matrix, new_norm, new_max.T)


def solution(mesh):
    torus = Mesh(mesh.devices.reshape(NZ, NY, NX, mesh.shape["tp"]), (*EP, "tp"))
    placed = (
        P(EP, None), P(), P(EP, "tp"), P(EP, "tp"), P(EP, "tp"), P(EP, "tp"), P(EP, "tp"),
        P(EP, "tp"), P("tp"), P("tp"), P("tp"), P("tp", EP), P(EP, "tp", None, None),
        P(EP, "tp", None), P(EP, "tp"), P(), P(EP, None, "tp"), P(EP, None, "tp"),
        P(EP, "tp", None), P(EP, None), P(EP, None),
    )
    return jax.shard_map(
        body,
        mesh=torus,
        in_specs=placed,
        out_specs=(P(EP, None), P(EP, "tp", None, None), P(EP, "tp", None), P(EP, "tp")),
        check_vma=False,
    )
```

time: 302 us -> 97 us (0.32)
  waiting for transfers between devices: 144 us -> 0 us
  Pallas kernels: 0 us -> 88.6 us
  blocking collectives: 79.1 us -> 0 us
  matrix products: 26.3 us -> 0 us
  between operations: 14.3 us -> 0.65 us
  local copies, waits for them, and re-layouts: 19.2 us -> 7.6 us
  other arithmetic: 10.8 us -> 0 us
  starting transfers between devices: 7.4 us -> 0 us
    all_gather x2 -> x0, waiting for transfers between devices: 115 us -> none  [the longest x1 95.9 us: sent_together(): filled, at, done = (lax.all_gather(both, axis, axis=dim, tiled=True), 0, [])]
    pallas_call x0 -> x1, Pallas kernels: none -> 88.6 us  [fused(): pl.pallas_call(fused_kernel, name='layer', out_shape=(jax.ShapeDtypeStruc...]
    all_to_all x3 -> x0, blocking collectives: 58.3 us -> none  [the longest x1 40 us: body(): lax.all_to_all(outgoing, EP, split_axis=0, concat_axis=0, tiled=True)]
    all_to_all x1 -> x0, waiting for transfers between devices: 29 us -> none  [body(): lax.all_to_all(finished, EP, split_axis=0, concat_axis=0, tiled=True)]
    dot_general x11 -> x0, matrix products: 26.3 us -> none  [the longest x5 7.95 us: body(): jnp.dot(normed, shard_piece, preferred_element_type=jnp.float32)]
    all_gather x2 -> x0, blocking collectives: 20.8 us -> none  [gathered_by_axis(): nearer = lax.all_gather(value, axes[-1], axis=dim, tiled=True)]
    all_to_all x1 -> x0, starting transfers between devices: 7.32 us -> none  [body(): lax.all_to_all(finished, EP, split_axis=0, concat_axis=0, tiled=True)]
    reshape x7 -> x0, local copies, waits for them, and re-layouts: 6.29 us -> none  [the longest x1 2.54 us: body(): outgoing = outgoing.reshape(expert_total, capacity, width)]
  transfers between devices with their start and end apart: 3 -> 0, of which waited for: 3 -> 0; matrix products, arithmetic and copies ran while one was open for 6% -> 0% of each run, Pallas kernels for 0% -> 0%
where the time goes in v2:
time: 97 us; the launch traced here: 96.9 us
  Pallas kernels  88.6 us (91%)
  local copies, waits for them, and re-layouts  7.6 us (8%)
    pallas_call x1, Pallas kernels, fused(): pl.pallas_call(fused_kernel, name='layer', out_shape=(jax.ShapeDtypeStruc...  88.6 us
    unnamed x8, local copies, waits for them, and re-layouts  7.6 us

profile of v2, /device:TPU:1, one launch (start us, length us, event | category | flops | bytes accessed | tf_op | source)
XLA Modules:
  0.0 96.9 jit_solution(4056749598607034833)
XLA Ops:
  0.6 88.6 %layer.1 = (bf16[32,2048]{1,0:T(8,128)(2,1)}, f32[32,4,64,64]{3,2,1,0:T(8,128)}, f32[32,4,64]{2,1,0:T(4,128)}, f32[4,32]{1,0:T(4,128)}) custom-call(bf16[32,2048]{1,0:T(8,128)(2,1)} %tok_h.1, f32[1,2048]{1,0:T(1,128)} %bitcast.16, bf16[16,256]{1,0:T(8,128)(2,1)} %wq_h.1, bf16[16,256]{1,0:T(8,128)(2,1)} %wk_h.1, bf16[16,256]{1,0:T(8,128)(2,1)} %wv_h.1, ...), custom_call_target="tpu_custom_call" | custom-call | tf_op jit(solution)/shard_map/layer/pallas_call | solution.py:496
  89.3 1.6 %copy.29 = bf16[32,2048]{1,0:T(8,128)(2,1)} copy(bf16[32,2048]{1,0:T(8,128)(2,1)} %get-tuple-element.16) | data formatting | bytes 262144
  90.8 0.0 copy-start
  90.8 0.0 copy-start.1
  90.8 4.8 %copy.30 = f32[32,4,64,64]{3,2,1,0:T(8,128)} copy(f32[32,4,64,64]{3,2,1,0:T(8,128)} %get-tuple-element.17) | data formatting | bytes 4194304
  95.7 0.0 copy-done
  95.7 0.6 copy.31
  96.3 0.0 copy-done.1
  96.3 0.6 copy.32
Async XLA Ops:
  90.8 4.8 %copy-start = (f32[32,4,64]{2,1,0:T(4,128)S(1)}, f32[32,4,64]{2,1,0:T(4,128)}, u32[]{:S(2)}) copy-start(f32[32,4,64]{2,1,0:T(4,128)} %get-tuple-element.18) | copy-start | bytes 98308
  90.8 5.5 %copy-start.1 = (f32[4,32]{1,0:T(4,128)S(1)}, f32[4,32]{1,0:T(4,128)}, u32[]{:S(2)}) copy-start(f32[4,32]{1,0:T(4,128)} %get-tuple-element.11) | copy-start | bytes 1540

commit v3 on v2

--- a/solution.py
+++ b/solution.py
@@ -49,17 +49,18 @@
 
 
 ZOFF = (4, 3, 5, 2, 6, 1, 7)
+OUTS = (((ROWS, D), BF16), ((ROWS, 4, 64, 64), F32), ((ROWS, 4, 64), F32), ((4, ROWS), F32))
 
 
 def fused_kernel(
     tok_h, mg_h, wq_h, wk_h, wv_h, wg_h, ig_h, fg_h, ib_h, fb_h, hg_h, wo_h, sm_h, sn_h, fgain_h,
     rt_h, rw_h, st_h, eg_h, eu_h, ed_h,
-    mixed_ref, nmat_h, nnorm_ref, nmax_ref,
+    mixed_ref, nmat_ref, nnorm_ref, nmax_ref,
     tok, mg, wq, wk, wv, wg, ig, fg, ib, fb, hg, wo, sm, sn, fgain, rt, rw, st, eg, eu, ed,
     nall, wst, gst, gtile, gsum, wfull, gt, woz, wof, res, proj, tbuf, b8,
     qrow, kcol, keep, scal, vt, cell,
     p_my, p_ot, resid, ntwo, amat, wmat, outt, rcv, xf, xm, hid, pd, pd_ot, own, yf, back, ret,
-    ld, out_sem, n_r, f_s, f_r, one_s, one_r, d_r, h_s, h_r, k_r, b_r,
+    ld, n_r, f_s, f_r, one_s, one_r, d_r, h_s, h_r, k_r, b_r,
 ):
     z, y, x, c = whereami()
     yx = y * NX + x
@@ -96,15 +97,14 @@
 
     barrier = pltpu.get_barrier_semaphore()
 
-    def greet_plane(off, lo):
-        def greet(j):
-            to, _ = place(off, j)
-            pl.semaphore_signal(barrier, 1, device_id=to, device_id_type=MESH)
-
-        loop(lo, NP, greet)
-
-    loop(1, NZ, lambda i: greet_plane(i, 0))
-    greet_plane(0, 1)
+    for d in ZOFF:
+        pl.semaphore_signal(barrier, 1, device_id=(zpeer(d), y, x, c), device_id_type=MESH)
+
+    def greet(d):
+        yt, xt, _ = ppeer(d)
+        pl.semaphore_signal(barrier, 1, device_id=(z, yt, xt, c), device_id_type=MESH)
+
+    loop(1, NP, greet)
     pl.semaphore_signal(barrier, 1, device_id=partner, device_id_type=MESH)
 
     for load in loads[:18]:
@@ -119,7 +119,7 @@
     tbuf[pl.ds(pl.multiple_of(z * 8, 8), 8), :] = b8[...]
     gtile[...] = tbuf[...].T[0:16, :].astype(BF16)
 
-    pl.semaphore_wait(barrier, NZ * NP)
+    pl.semaphore_wait(barrier, NZ - 1 + NP - 1 + 1)
 
     wsrc = (wq, wk, wv, wg)
 
@@ -151,9 +151,9 @@
     for d in ZOFF:
         gz_send(d).start()
     for d in ZOFF:
+        o_send(d).start()
+    for d in ZOFF:
         n_send(d).start()
-    for d in ZOFF:
-        o_send(d).start()
     gst[z] = gtile[...]
     woz[z] = wo[...]
 
@@ -187,6 +187,11 @@
 
     loop(1, NP, lambda d: x_send(d).start())
     loop(1, NP, lambda d: g_send(d).start())
+
+    arrived(woz.at[0:7], one_r.at[2])
+    for k in range(NZ):
+        wof[k, yx] = woz[k]
+    loop(1, NP, lambda d: v_send(d).start())
 
     tbuf[...] = jnp.zeros((128, 128), F32)
     tbuf[0:3, 0:32] = rt[...].astype(F32)
@@ -227,11 +232,6 @@
         wmat[0:256, at] = high
         wmat[256:512, at] = (weight - high.astype(F32)).astype(BF16)
 
-    arrived(woz.at[0:7], one_r.at[2])
-    for k in range(NZ):
-        wof[k, yx] = woz[k]
-    loop(1, NP, lambda d: v_send(d).start())
-
     def f_send(zs):
         return push(nall.at[zs, :, half], nall.at[zs, :, half], f_s, f_r.at[zs], partner)
 
@@ -383,11 +383,9 @@
                 lax.broadcasted_iota(jnp.int32, (64, ROWS), 1) == b, vth.astype(F32), 0.0
             ).astype(BF16)
             outer = nn_dot(pick, kcol[h])
-            st[b, h] = keep[h, pl.ds(b, 1), :] * st[b, h] + scal[h, pl.ds(b, 1), :] * outer
+            nmat_ref[b, h] = keep[h, pl.ds(b, 1), :] * st[b, h] + scal[h, pl.ds(b, 1), :] * outer
 
     loop(0, ROWS, write_one)
-    save = pltpu.make_async_copy(st, nmat_h, out_sem)
-    save.start()
 
     def h_view(s, zs):
         return rcv.at[s, plane16(zs)]
@@ -479,15 +477,37 @@
     left(back.at[0:127], one_s.at[11])
     left(nall.at[0:7, :, half], f_s)
     left(outt, h_s)
-    save.wait()
     arrived(mixed_ref.at[:, other], one_r.at[12])
     last.wait_send()
+
+
+def store_kernel(*refs):
+    n = len(OUTS)
+    sems = refs[-1]
+    moves = [pltpu.make_async_copy(refs[k], refs[n + k], sems.at[k]) for k in range(n)]
+    for move in moves:
+        move.start()
+    for move in moves:
+        move.wait()
+
+
+def stored(*arrays):
+    n = len(OUTS)
+    return pl.pallas_call(
+        store_kernel,
+        name="store",
+        out_shape=tuple(jax.ShapeDtypeStruct(shape, kind) for shape, kind in OUTS),
+        in_specs=[pl.BlockSpec(memory_space=pltpu.VMEM)] * n,
+        out_specs=(pl.BlockSpec(memory_space=pl.ANY),) * n,
+        scratch_shapes=[pltpu.SemaphoreType.DMA((n,))],
+        compiler_params=pltpu.CompilerParams(vmem_limit_bytes=8 << 20),
+    )(*arrays)
 
 
 def fused(*args):
     dma = pltpu.SemaphoreType.DMA
     vm = pl.BlockSpec(memory_space=pltpu.VMEM)
-    hbm = pl.BlockSpec(memory_space=pl.ANY)
+    hbm = pl.BlockSpec(memory_space=pltpu.HBM)
 
     def buf(shape, kind=BF16):
         return pltpu.VMEM(shape, kind)
@@ -496,14 +516,9 @@
     return pl.pallas_call(
         fused_kernel,
         name="layer",
-        out_shape=(
-            jax.ShapeDtypeStruct((ROWS, D), BF16),
-            jax.ShapeDtypeStruct((ROWS, 4, 64, 64), F32),
-            jax.ShapeDtypeStruct((ROWS, 4, 64), F32),
-            jax.ShapeDtypeStruct((4, ROWS), F32),
-        ),
+        out_shape=tuple(pltpu.VMEM(shape, kind) for shape, kind in OUTS),
         in_specs=[hbm] * len(args),
-        out_specs=(vm, hbm, vm, vm),
+        out_specs=(vm, vm, vm, vm),
         scratch_shapes=[
             *staged,
             buf((NZ, ROWS, D)),
@@ -543,7 +558,6 @@
             buf((128, 16, 128)),
             buf((128, 16, 128)),
             dma((len(args),)),
-            dma,
             dma((NZ,)),
             dma,
             dma((NZ,)),
@@ -556,20 +570,20 @@
             dma((NZ,)),
         ],
         compiler_params=pltpu.CompilerParams(
-            collective_id=0, has_side_effects=True, vmem_limit_bytes=58 << 20
+            collective_id=0, has_side_effects=True, vmem_limit_bytes=40 << 20
         ),
-    )(*args)
+    )(*(pltpu.with_memory_space_constraint(a, pltpu.HBM) for a in args))
 
 
 def body(tokens, mix_gain, w_query, w_key, w_value, w_outgate, w_igate, w_fgate, igate_bias,
          fgate_bias, head_gain, w_out, state_matrix, state_norm, state_max, ffn_gain,
          w_expert_gate, w_expert_up, w_expert_down, routes, route_weights):
-    mixed, new_matrix, new_norm, new_max = fused(
+    mixed, new_matrix, new_norm, new_max = stored(*fused(
         tokens, mix_gain.reshape(1, D), w_query, w_key, w_value, w_outgate, w_igate.T, w_fgate.T,
         igate_bias.reshape(1, 4), fgate_bias.reshape(1, 4), head_gain.reshape(1, 256), w_out.T,
         state_max.T, state_norm, ffn_gain.reshape(1, D), routes.T, route_weights.T, state_matrix,
         w_expert_gate.swapaxes(1, 2), w_expert_up.swapaxes(1, 2), w_expert_down,
-    )
+    ))
     return (mixed, new_matrix, new_norm, new_max.T)
 
 

time: 97 us -> 82.9 us (0.85)
  local copies, waits for them, and re-layouts: 7.6 us -> 0 us
  Pallas kernels: 88.6 us -> 82.1 us
    unnamed x8 -> x0, local copies, waits for them, and re-layouts: 7.6 us -> none
    pallas_call x1 -> x2, Pallas kernels: 88.6 us -> 82.1 us  [the longest x1 80 us: fused(): pl.pallas_call(fused_kernel, name='layer', out_shape=tuple((pltpu.VMEM(sh...]
where the time goes in v3:
time: 82.9 us; the launch traced here: 82.8 us
  Pallas kernels  82.1 us (99%)
    pallas_call x1, Pallas kernels, fused(): pl.pallas_call(fused_kernel, name='layer', out_shape=tuple((pltpu.VMEM(sh...  80 us
    pallas_call x1, Pallas kernels, stored(): pl.pallas_call(store_kernel, name='store', out_shape=tuple((jax.ShapeDtyp...  2.1 us

profile of v3, /device:TPU:1, one launch (start us, length us, event | category | flops | bytes accessed | tf_op | source)
XLA Modules:
  0.0 82.8 jit_solution(12970459029218708909)
XLA Ops:
  0.6 80.0 %layer.1 = (bf16[32,2048]{1,0:T(8,128)(2,1)S(1)}, f32[32,4,64,64]{3,2,1,0:T(8,128)S(1)}, f32[32,4,64]{2,1,0:T(4,128)S(1)}, f32[4,32]{1,0:T(4,128)S(1)}) custom-call(bf16[32,2048]{1,0:T(8,128)(2,1)} %tok_h.1, f32[1,2048]{1,0:T(1,128)} %bitcast.16, bf16[16,256]{1,0:T(8,128)(2,1)} %wq_h.1, bf16[16,256]{1,0:T(8,128)(2,1)} %wk_h.1, bf16[16,256]{1,0:T(8,128)(2,1)} %wv_h.1, ...), custom_call_target="tpu_custom_call" | custom-call | tf_op jit(solution)/shard_map/layer/pallas_call | solution.py:516
  80.7 2.1 %store.1 = (bf16[32,2048]{1,0:T(8,128)(2,1)}, f32[32,4,64,64]{3,2,1,0:T(8,128)}, f32[32,4,64]{2,1,0:T(4,128)}, f32[4,32]{1,0:T(4,128)}) custom-call(bf16[32,2048]{1,0:T(8,128)(2,1)S(1)} %get-tuple-element.12.refs_0_, f32[32,4,64,64]{3,2,1,0:T(8,128)S(1)} %get-tuple-element.13.refs_1_, f32[32,4,64]{2,1,0:T(4,128)S(1)} %get-tuple-element.14.refs_2_, ...), custom_call_target="tpu_custom_call" | custom-call | tf_op jit(solution)/shard_map/store/pallas_call | solution.py:496

commit v4 on v3

--- a/solution.py
+++ b/solution.py
@@ -49,7 +49,8 @@
 
 
 ZOFF = (4, 3, 5, 2, 6, 1, 7)
-OUTS = (((ROWS, D), BF16), ((ROWS, 4, 64, 64), F32), ((ROWS, 4, 64), F32), ((4, ROWS), F32))
+JOFF = (10, 9, 11, 6, 14, 2, 8, 5, 7, 13, 15, 1, 3, 4, 12, 0)
+OUTS = (((ROWS, D), BF16), ((ROWS * 256, 64), F32), ((ROWS, 4, 64), F32), ((4, ROWS), F32))
 
 
 def fused_kernel(
@@ -57,10 +58,10 @@
     rt_h, rw_h, st_h, eg_h, eu_h, ed_h,
     mixed_ref, nmat_ref, nnorm_ref, nmax_ref,
     tok, mg, wq, wk, wv, wg, ig, fg, ib, fb, hg, wo, sm, sn, fgain, rt, rw, st, eg, eu, ed,
-    nall, wst, gst, gtile, gsum, wfull, gt, woz, wof, res, proj, tbuf, b8,
+    stt, nall, wst, gst, gtile, gsum, wfull, gt, woz, wof, res, proj, tbuf, b8,
     qrow, kcol, keep, scal, vt, cell,
-    p_my, p_ot, resid, ntwo, amat, wmat, outt, rcv, xf, xm, hid, pd, pd_ot, own, yf, back, ret,
-    ld, n_r, f_s, f_r, one_s, one_r, d_r, h_s, h_r, k_r, b_r,
+    p_my, p_ot, resid, ntwo, amat, wmat, outt, rcv, xf, xm, ga, ua, hid, pd, pd_ot, own, yf, back, ret,
+    ld, n_r, n4_r, f_s, f_r, one_s, one_r, d_r, h_s, h_r, k_r, b_r,
 ):
     z, y, x, c = whereami()
     yx = y * NX + x
@@ -90,10 +91,23 @@
 
         lax.fori_loop(lo, hi, step, 0)
 
-    def place(off, j):
-        zt = zpeer(off)
-        yt, xt, yxt = ppeer(j)
-        return (zt, yt, xt, c), zt * NP + yxt
+    spots = [ppeer(j) for j in range(NP)]
+
+    def planes(body):
+        def step(i, carry):
+            body(i, zpeer(4 + (1 - 2 * (i % 2)) * ((i + 1) // 2)))
+            return carry
+
+        lax.fori_loop(0, NZ, step, 0)
+
+    def send_plane(i, zt, send):
+        for j in JOFF:
+            yt, xt, yxt = spots[j]
+            copy = send((zt, yt, xt, c), zt * NP + yxt)
+            if j:
+                copy.start()
+            else:
+                pl.when(i < NZ - 1)(copy.start)
 
     barrier = pltpu.get_barrier_semaphore()
 
@@ -107,7 +121,7 @@
     loop(1, NP, greet)
     pl.semaphore_signal(barrier, 1, device_id=partner, device_id_type=MESH)
 
-    for load in loads[:18]:
+    for load in loads[:17]:
         load.wait()
 
     nall[z] = rms_scale(tok[...].astype(F32), mg[...]).astype(BF16)
@@ -148,11 +162,22 @@
         return push(nall.at[z, :, half], nall.at[z, :, half], one_s.at[3], n_r.at[z],
                     (zpeer(d), y, x, c))
 
+    def quarter(part):
+        return pl.ds(pl.multiple_of(c * HALF + part * (HALF // 2), HALF // 2), HALF // 2)
+
+    def relay(side):
+        zs = zpeer(NZ - 2 * side)
+        part = quarter(0 if side > 0 else 1)
+        view, cut = nall.at[zs, :, half], nall.at[zs, :, part]
+        n4 = n_r.at[zs] if side > 0 else n4_r
+        push(view, view, one_s.at[13], n_r.at[zs], (zpeer(NZ + side), y, x, c)).start()
+        push(cut, cut, one_s.at[14], n4, (zpeer(NZ + 2 * side), y, x, c)).start()
+
     for d in ZOFF:
         gz_send(d).start()
     for d in ZOFF:
         o_send(d).start()
-    for d in ZOFF:
+    for d in (2, 6, 1, 7):
         n_send(d).start()
     gst[z] = gtile[...]
     woz[z] = wo[...]
@@ -187,6 +212,15 @@
 
     loop(1, NP, lambda d: x_send(d).start())
     loop(1, NP, lambda d: g_send(d).start())
+
+    def f_send(zs):
+        return push(nall.at[zs, :, half], nall.at[zs, :, half], f_s, f_r.at[zs], partner)
+
+    for side in (1, -1):
+        zs = zpeer(NZ - 2 * side)
+        arrived(nall.at[zs, :, half], n_r.at[zs])
+        relay(side)
+        f_send(zs).start()
 
     arrived(woz.at[0:7], one_r.at[2])
     for k in range(NZ):
@@ -232,12 +266,21 @@
         wmat[0:256, at] = high
         wmat[256:512, at] = (weight - high.astype(F32)).astype(BF16)
 
-    def f_send(zs):
-        return push(nall.at[zs, :, half], nall.at[zs, :, half], f_s, f_r.at[zs], partner)
-
-    for d in (1, 7, 2, 6, 3, 5, 4):
+    loads[17].wait()
+
+    def turn(v):
+        heads = [st[pl.ds(h * 64 + v, ROWS, stride=256), :] for h in range(4)]
+        stt[v] = jnp.concatenate(heads, axis=0).T
+
+    lax.fori_loop(0, 64, lambda v, carry: (turn(v), carry)[1], 0, unroll=4)
+
+    for d in (1, 7, 3, 5, 4):
         zs = zpeer(d)
-        arrived(nall.at[zs, :, half], n_r.at[zs])
+        if d == 4:
+            arrived(nall.at[zs, :, quarter(0)], n_r.at[zs])
+            arrived(nall.at[zs, :, quarter(1)], n4_r)
+        else:
+            arrived(nall.at[zs, :, half], n_r.at[zs])
         f_send(zs).start()
 
     arrived(gt.at[0:15], one_r.at[5])
@@ -305,16 +348,10 @@
             keep[n] = jnp.broadcast_to(keep_old[:, n:n + 1], (ROWS, 64))
             scal[n] = jnp.broadcast_to(keep_new[:, n:n + 1] * 0.125, (ROWS, 64))
 
-    lane64 = lax.broadcasted_iota(jnp.int32, (64, 128), 1)
-
-    def read_one(b, acc):
-        done = []
-        for h in range(4):
-            prod = st[b, h] * qrow[h, pl.ds(b, 1), :]
-            done.append(jnp.where(lane64 == b, jnp.sum(prod, axis=1, keepdims=True), acc[h]))
-        return tuple(done)
-
-    acc = lax.fori_loop(0, ROWS, read_one, tuple(jnp.zeros((64, 128), F32) for _ in range(4)))
+    q_t = jnp.concatenate([qrow[h] for h in range(4)], axis=0).T
+    for k in range(8):
+        tbuf[8 * k:8 * k + 8, :] = jnp.sum(stt[8 * k:8 * k + 8] * q_t[None], axis=1)
+    num = tbuf[0:64, :].T
 
     for p in range(2):
         q, kk, vv = proj[p].astype(F32), proj[2 + p].astype(F32) * 0.125, proj[4 + p].astype(F32)
@@ -325,9 +362,9 @@
             return v[:, h0:h0 + 1], v[:, h1:h1 + 1]
 
         ko, kn = two(keep_old), two(keep_new)
-        tbuf[0:64, :] = acc[h0]
-        tbuf[64:128, :] = acc[h1]
-        num0 = tbuf[...].T[0:ROWS, :]
+        num0 = jnp.concatenate(
+            [num[ROWS * h0:ROWS * (h0 + 1)], num[ROWS * h1:ROWS * (h1 + 1)]], axis=1
+        )
         norm_in = jnp.concatenate([sn[:, h0, :], sn[:, h1, :]], axis=1)
         norm_new = spread(ko) * norm_in + spread(kn) * kk
         nnorm_ref[:, h0, :] = norm_new[:, 0:64]
@@ -359,8 +396,7 @@
 
     xr = jnp.concatenate([ntwo[:, cols(c, k)] for k in range(8)], axis=0)
 
-    def d_send(off, j):
-        to, e = place(off, j)
+    def d_send(to, e):
         return push(outt.at[e], rcv.at[c, me], one_s.at[9], d_r.at[z], to)
 
     def plane256(zt):
@@ -369,11 +405,12 @@
     def plane16(zt):
         return pl.ds(zt * NP, NP)
 
-    for off in (*ZOFF, 0):
-        zt = zpeer(off)
+    def dispatch(i, zt):
         rows = nn_dot(amat[plane256(zt), :], xr).astype(BF16)
         outt[plane16(zt)] = rows.reshape(NP, 16, 128)
-        loop(1 if off == 0 else 0, NP, lambda j, off=off: d_send(off, j).start())
+        send_plane(i, zt, d_send)
+
+    planes(dispatch)
     rcv[c, me] = outt[me]
 
     def write_one(b):
@@ -383,7 +420,8 @@
                 lax.broadcasted_iota(jnp.int32, (64, ROWS), 1) == b, vth.astype(F32), 0.0
             ).astype(BF16)
             outer = nn_dot(pick, kcol[h])
-            nmat_ref[b, h] = keep[h, pl.ds(b, 1), :] * st[b, h] + scal[h, pl.ds(b, 1), :] * outer
+            at = pl.ds(pl.multiple_of((b * 4 + h) * 64, 64), 64)
+            nmat_ref[at, :] = keep[h, pl.ds(b, 1), :] * st[at, :] + scal[h, pl.ds(b, 1), :] * outer
 
     loop(0, ROWS, write_one)
 
@@ -407,17 +445,22 @@
             arrived(rcv.at[c, 0:15], d_r.at[zs])
         h_send(zs).start()
         unpack(c, zs)
+    for load in loads[18:]:
+        load.wait()
+
+    parts = ((0, 256), (256, 512), (512, DE))
+    for lo, hi in parts:
+        ga[:, lo:hi] = nt_dot(xm[:, half], eg[lo:hi, half])
+        ua[:, lo:hi] = nt_dot(xm[:, half], eu[lo:hi, half])
+
     for off in (*ZOFF, 0):
         zs = (z + NZ - off) % NZ
         arrived(h_view(1 - c, zs), h_r.at[zs])
         unpack(1 - c, zs)
 
-    for load in loads[18:]:
-        load.wait()
-
-    for lo, hi in ((0, 256), (256, 512), (512, DE)):
-        gate = nt_dot(xm[...], eg[lo:hi, :])
-        up = nt_dot(xm[...], eu[lo:hi, :])
+    for lo, hi in parts:
+        gate = ga[:, lo:hi] + nt_dot(xm[:, other], eg[lo:hi, other])
+        up = ua[:, lo:hi] + nt_dot(xm[:, other], eu[lo:hi, other])
         hid[:, lo:hi] = (gate * jax.nn.sigmoid(gate) * up).astype(BF16)
 
     def down(s, k):
@@ -437,14 +480,14 @@
         for h in range(2):
             yf[pl.ds(2 * k + h, 256, stride=8), :] = both[:, 128 * h:128 * (h + 1)]
 
-    def b_send(off, j):
-        to, s = place(off, j)
+    def b_send(to, s):
         return push(back.at[s], ret.at[me], one_s.at[11], b_r.at[z], to)
 
-    for off in (*ZOFF, 0):
-        zt = zpeer(off)
+    def give_back(i, zt):
         back[plane16(zt)] = yf[plane256(zt), :].astype(BF16).reshape(NP, 16, 128)
-        loop(1 if off == 0 else 0, NP, lambda j, off=off: b_send(off, j).start())
+        send_plane(i, zt, b_send)
+
+    planes(give_back)
     ret[me] = back[me]
 
     weighted = jnp.zeros((512, 128), F32)
@@ -466,7 +509,9 @@
     left(wst.at[0:7], one_s.at[0])
     left(gst.at[0:7], one_s.at[1])
     left(woz.at[0:7], one_s.at[2])
-    left(nall.at[0:7, :, half], one_s.at[3])
+    left(nall.at[0:4, :, half], one_s.at[3])
+    left(nall.at[0:2, :, half], one_s.at[13])
+    left(nall.at[0:1, :, half], one_s.at[14])
     left(wfull.at[:, 0:15], one_s.at[4])
     left(gt.at[0:15], one_s.at[5])
     left(wof.at[:, 0:15], one_s.at[6])
@@ -481,10 +526,16 @@
     last.wait_send()
 
 
+PIECES = 8
+
+
 def store_kernel(*refs):
     n = len(OUTS)
     sems = refs[-1]
-    moves = [pltpu.make_async_copy(refs[k], refs[n + k], sems.at[k]) for k in range(n)]
+    step = ROWS * 256 // PIECES
+    pairs = [(refs[1].at[k * step:(k + 1) * step], refs[n + 1].at[k * step:(k + 1) * step]) for k in range(PIECES)]
+    pairs += [(refs[k], refs[n + k]) for k in (0, 2, 3)]
+    moves = [pltpu.make_async_copy(a, b, sems.at[k]) for k, (a, b) in enumerate(pairs)]
     for move in moves:
         move.start()
     for move in moves:
@@ -499,7 +550,7 @@
         out_shape=tuple(jax.ShapeDtypeStruct(shape, kind) for shape, kind in OUTS),
         in_specs=[pl.BlockSpec(memory_space=pltpu.VMEM)] * n,
         out_specs=(pl.BlockSpec(memory_space=pl.ANY),) * n,
-        scratch_shapes=[pltpu.SemaphoreType.DMA((n,))],
+        scratch_shapes=[pltpu.SemaphoreType.DMA((n - 1 + PIECES,))],
         compiler_params=pltpu.CompilerParams(vmem_limit_bytes=8 << 20),
     )(*arrays)
 
@@ -521,6 +572,7 @@
         out_specs=(vm, vm, vm, vm),
         scratch_shapes=[
             *staged,
+            buf((64, 64, 128), F32),
             buf((NZ, ROWS, D)),
             buf((NZ, 16, 128)),
             buf((NZ, 16, 128)),
@@ -550,6 +602,8 @@
             buf((2, 128, 16, 128)),
             buf((256, 128), F32),
             buf((256, D)),
+            buf((256, DE), F32),
+            buf((256, DE), F32),
             buf((256, DE)),
             buf((4, 256, 256)),
             buf((4, 256, 256)),
@@ -560,9 +614,10 @@
             dma((len(args),)),
             dma((NZ,)),
             dma,
+            dma,
             dma((NZ,)),
-            dma((13,)),
-            dma((13,)),
+            dma((15,)),
+            dma((15,)),
             dma((NZ,)),
             dma,
             dma((NZ,)),
@@ -581,10 +636,10 @@
     mixed, new_matrix, new_norm, new_max = stored(*fused(
         tokens, mix_gain.reshape(1, D), w_query, w_key, w_value, w_outgate, w_igate.T, w_fgate.T,
         igate_bias.reshape(1, 4), fgate_bias.reshape(1, 4), head_gain.reshape(1, 256), w_out.T,
-        state_max.T, state_norm, ffn_gain.reshape(1, D), routes.T, route_weights.T, state_matrix,
+        state_max.T, state_norm, ffn_gain.reshape(1, D), routes.T, route_weights.T, state_matrix.reshape(ROWS * 256, 64),
         w_expert_gate.swapaxes(1, 2), w_expert_up.swapaxes(1, 2), w_expert_down,
     ))
-    return (mixed, new_matrix, new_norm, new_max.T)
+    return (mixed, new_matrix.reshape(ROWS, 4, 64, 64), new_norm, new_max.T)
 
 
 def solution(mesh):

time: 82.9 us -> 78.7 us (0.949)
  Pallas kernels: 82.1 us -> 77.9 us
    pallas_call x1, Pallas kernels: 80 us -> 75.8 us  [fused(): pl.pallas_call(fused_kernel, name='layer', out_shape=tuple((pltpu.VMEM(sh...]
where the time goes in v4:
time: 78.7 us; the launch traced here: 78.6 us
  Pallas kernels  77.9 us (99%)
    pallas_call x1, Pallas kernels, fused(): pl.pallas_call(fused_kernel, name='layer', out_shape=tuple((pltpu.VMEM(sh...  75.8 us
    pallas_call x1, Pallas kernels, stored(): pl.pallas_call(store_kernel, name='store', out_shape=tuple((jax.ShapeDtyp...  2.15 us

profile of v4, /device:TPU:1, one launch (start us, length us, event | category | flops | bytes accessed | tf_op | source)
XLA Modules:
  0.0 78.6 jit_solution(5708825817711079696)
XLA Ops:
  0.6 75.8 %layer.1 = (bf16[32,2048]{1,0:T(8,128)(2,1)S(1)}, f32[8192,64]{1,0:T(8,128)S(1)}, f32[32,4,64]{2,1,0:T(4,128)S(1)}, f32[4,32]{1,0:T(4,128)S(1)}) custom-call(bf16[32,2048]{1,0:T(8,128)(2,1)} %tok_h.1, f32[1,2048]{1,0:T(1,128)} %bitcast.19, bf16[16,256]{1,0:T(8,128)(2,1)} %wq_h.1, bf16[16,256]{1,0:T(8,128)(2,1)} %wk_h.1, bf16[16,256]{1,0:T(8,128)(2,1)} %wv_h.1, ...), custom_call_target="tpu_custom_call" | custom-call | tf_op jit(solution)/shard_map/layer/pallas_call | solution.py:567
  76.4 2.1 %store.1 = (bf16[32,2048]{1,0:T(8,128)(2,1)}, f32[8192,64]{1,0:T(8,128)}, f32[32,4,64]{2,1,0:T(4,128)}, f32[4,32]{1,0:T(4,128)}) custom-call(bf16[32,2048]{1,0:T(8,128)(2,1)S(1)} %get-tuple-element.12.refs_0_, f32[8192,64]{1,0:T(8,128)S(1)} %get-tuple-element.13.refs_1_, f32[32,4,64]{2,1,0:T(4,128)S(1)} %get-tuple-element.14.refs_2_, ...), custom_call_target="tpu_custom_call" | custom-call | tf_op jit(solution)/shard_map/store/pallas_call | solution.py:547

commit v5 on v4

--- a/solution.py
+++ b/solution.py
@@ -58,10 +58,10 @@
     rt_h, rw_h, st_h, eg_h, eu_h, ed_h,
     mixed_ref, nmat_ref, nnorm_ref, nmax_ref,
     tok, mg, wq, wk, wv, wg, ig, fg, ib, fb, hg, wo, sm, sn, fgain, rt, rw, st, eg, eu, ed,
-    stt, nall, wst, gst, gtile, gsum, wfull, gt, woz, wof, res, proj, tbuf, b8,
+    stt, nall, wst, gst, gtile, gsum, wfull, gt, woz, wof, wofb, res, proj, tbuf, b8,
     qrow, kcol, keep, scal, vt, cell,
     p_my, p_ot, resid, ntwo, amat, wmat, outt, rcv, xf, xm, ga, ua, hid, pd, pd_ot, own, yf, back, ret,
-    ld, n_r, n4_r, f_s, f_r, one_s, one_r, d_r, h_s, h_r, k_r, b_r,
+    ld, n_r, e_r, e4_r, f_s, f_r, one_s, one_r, d_r, h_s, h_r, k_r, b_r,
 ):
     z, y, x, c = whereami()
     yx = y * NX + x
@@ -156,76 +156,57 @@
         return push(gtile, gst.at[z], one_s.at[1], one_r.at[1], (zpeer(d), y, x, c))
 
     def o_send(d):
-        return push(wo, woz.at[z], one_s.at[2], one_r.at[2], (zpeer(d), y, x, c))
-
-    def n_send(d):
-        return push(nall.at[z, :, half], nall.at[z, :, half], one_s.at[3], n_r.at[z],
-                    (zpeer(d), y, x, c))
+        return push(wo.at[:, 0:128], woz.at[z], one_s.at[2], one_r.at[2], (zpeer(d), y, x, c))
+
+    def e_send(d):
+        yt, xt, _ = ppeer(d)
+        return push(wo.at[:, 128:256], wofb.at[z, yx], one_s.at[15], one_r.at[15], (z, yt, xt, c))
+
+    def eb_send(d):
+        return push(wofb.at[z], wofb.at[z], one_s.at[16], e_r.at[z], (zpeer(d), y, x, c))
+
+    def eb_relay(side):
+        zs = zpeer(NZ - 2 * side)
+        view = wofb.at[zs]
+        cut = wofb.at[zs, 0:8] if side > 0 else wofb.at[zs, 8:16]
+        e4 = e_r.at[zs] if side > 0 else e4_r
+        push(view, view, one_s.at[17], e_r.at[zs], (zpeer(NZ + side), y, x, c)).start()
+        push(cut, cut, one_s.at[18], e4, (zpeer(NZ + 2 * side), y, x, c)).start()
+
+    def n_send(d, part):
+        view = nall.at[z, :, quarter(part)]
+        return push(view, view, one_s.at[3], n_r.at[part, z], (zpeer(d), y, x, c))
 
     def quarter(part):
         return pl.ds(pl.multiple_of(c * HALF + part * (HALF // 2), HALF // 2), HALF // 2)
 
-    def relay(side):
+    def relay(side, part):
         zs = zpeer(NZ - 2 * side)
-        part = quarter(0 if side > 0 else 1)
-        view, cut = nall.at[zs, :, half], nall.at[zs, :, part]
-        n4 = n_r.at[zs] if side > 0 else n4_r
-        push(view, view, one_s.at[13], n_r.at[zs], (zpeer(NZ + side), y, x, c)).start()
-        push(cut, cut, one_s.at[14], n4, (zpeer(NZ + 2 * side), y, x, c)).start()
-
+        view = nall.at[zs, :, quarter(part)]
+        push(view, view, one_s.at[13], n_r.at[part, zs], (zpeer(NZ + side), y, x, c)).start()
+        if (side > 0) == (part == 0):
+            push(view, view, one_s.at[14], n_r.at[part, zs], (zpeer(NZ + 2 * side), y, x, c)).start()
+
+    for part in range(2):
+        for d in (2, 6):
+            n_send(d, part).start()
+    for d in (1, 7):
+        for part in range(2):
+            n_send(d, part).start()
     for d in ZOFF:
         gz_send(d).start()
     for d in ZOFF:
         o_send(d).start()
-    for d in (2, 6, 1, 7):
-        n_send(d).start()
+    loop(1, NP, lambda d: e_send(d).start())
     gst[z] = gtile[...]
-    woz[z] = wo[...]
+    woz[z] = wo[:, 0:128]
+    wofb[z, yx] = wo[:, 128:256]
 
     def arrived(view, recv_sem):
         push(view, view, recv_sem, recv_sem, partner).wait_recv()
 
     def left(view, send_sem):
         push(view, view, send_sem, send_sem, partner).wait_send()
-
-    arrived(wst.at[0:7], one_r.at[0])
-    arrived(gst.at[0:7], one_r.at[1])
-    total = gst[0].astype(F32)
-    for k in range(1, NZ):
-        total = total + gst[k].astype(F32)
-    gsum[...] = total.astype(BF16)
-    gt[yx] = gsum[...]
-    for k in range(NZ):
-        wfull[k, yx] = wst[k]
-
-    def x_send(d):
-        yt, xt, _ = ppeer(d)
-        return push(wst, wfull.at[:, yx], one_s.at[4], one_r.at[4], (z, yt, xt, c))
-
-    def g_send(d):
-        yt, xt, _ = ppeer(d)
-        return push(gsum, gt.at[yx], one_s.at[5], one_r.at[5], (z, yt, xt, c))
-
-    def v_send(d):
-        yt, xt, _ = ppeer(d)
-        return push(woz, wof.at[:, yx], one_s.at[6], one_r.at[6], (z, yt, xt, c))
-
-    loop(1, NP, lambda d: x_send(d).start())
-    loop(1, NP, lambda d: g_send(d).start())
-
-    def f_send(zs):
-        return push(nall.at[zs, :, half], nall.at[zs, :, half], f_s, f_r.at[zs], partner)
-
-    for side in (1, -1):
-        zs = zpeer(NZ - 2 * side)
-        arrived(nall.at[zs, :, half], n_r.at[zs])
-        relay(side)
-        f_send(zs).start()
-
-    arrived(woz.at[0:7], one_r.at[2])
-    for k in range(NZ):
-        wof[k, yx] = woz[k]
-    loop(1, NP, lambda d: v_send(d).start())
 
     tbuf[...] = jnp.zeros((128, 128), F32)
     tbuf[0:3, 0:32] = rt[...].astype(F32)
@@ -266,23 +247,90 @@
         wmat[0:256, at] = high
         wmat[256:512, at] = (weight - high.astype(F32)).astype(BF16)
 
+    arrived(wst.at[0:7], one_r.at[0])
+    for k in range(NZ):
+        wfull[k, yx] = wst[k]
+
+    def x_send(d):
+        yt, xt, _ = ppeer(d)
+        return push(wst, wfull.at[:, yx], one_s.at[4], one_r.at[4], (z, yt, xt, c))
+
+    def g_send(d):
+        yt, xt, _ = ppeer(d)
+        return push(gsum, gt.at[yx], one_s.at[5], one_r.at[5], (z, yt, xt, c))
+
+    def v_send(d):
+        yt, xt, _ = ppeer(d)
+        return push(woz, wof.at[:, yx], one_s.at[6], one_r.at[6], (z, yt, xt, c))
+
+    loop(1, NP, lambda d: x_send(d).start())
+
+    def f_send(zs):
+        return push(nall.at[zs, :, half], nall.at[zs, :, half], f_s, f_r.at[zs], partner)
+
+    for part in range(2):
+        for side in (1, -1):
+            zs = zpeer(NZ - 2 * side)
+            arrived(nall.at[zs, :, quarter(part)], n_r.at[part, zs])
+            relay(side, part)
+    for d in (2, 6):
+        f_send(zpeer(d)).start()
+
+    def token_in(d):
+        zs = zpeer(d)
+        for part in range(2):
+            arrived(nall.at[zs, :, quarter(part)], n_r.at[part, zs])
+        f_send(zs).start()
+
+    for d in (1, 7):
+        token_in(d)
     loads[17].wait()
 
     def turn(v):
         heads = [st[pl.ds(h * 64 + v, ROWS, stride=256), :] for h in range(4)]
         stt[v] = jnp.concatenate(heads, axis=0).T
 
-    lax.fori_loop(0, 64, lambda v, carry: (turn(v), carry)[1], 0, unroll=4)
-
-    for d in (1, 7, 3, 5, 4):
+    def turns(lo, hi):
+        lax.fori_loop(lo, hi, lambda v, carry: (turn(v), carry)[1], 0, unroll=4)
+
+    turns(0, 32)
+
+    arrived(gst.at[0:7], one_r.at[1])
+    total = gst[0].astype(F32)
+    for k in range(1, NZ):
+        total = total + gst[k].astype(F32)
+    gsum[...] = total.astype(BF16)
+    gt[yx] = gsum[...]
+    loop(1, NP, lambda d: g_send(d).start())
+    arrived(woz.at[0:7], one_r.at[2])
+    for k in range(NZ):
+        wof[k, yx] = woz[k]
+    loop(1, NP, lambda d: v_send(d).start())
+
+    arrived(wofb.at[0, 0:15], one_r.at[15])
+    for d in (2, 6, 1, 7):
+        eb_send(d).start()
+
+    for d in (3, 5, 4):
+        token_in(d)
+
+    turns(32, 64)
+
+    for d in (1, 7, 2, 6, 3, 5, 4):
         zs = zpeer(d)
-        if d == 4:
-            arrived(nall.at[zs, :, quarter(0)], n_r.at[zs])
-            arrived(nall.at[zs, :, quarter(1)], n4_r)
-        else:
-            arrived(nall.at[zs, :, half], n_r.at[zs])
-        f_send(zs).start()
-
+        arrived(nall.at[zs, :, other], f_r.at[zs])
+    arrived(wfull.at[:, 0:15], one_r.at[4])
+
+    every = nn_dot(nall[...].reshape(NZ * ROWS, D), wfull[...].reshape(D, 128))
+    res[...] = every.astype(BF16).reshape(NZ, ROWS, 128)
+
+    def p_send(d):
+        zt = zpeer(d)
+        return push(res.at[zt], proj.at[z], one_s.at[7], one_r.at[7], (zt, y, x, c))
+
+    for d in ZOFF:
+        p_send(d).start()
+    proj[z] = res[z]
     arrived(gt.at[0:15], one_r.at[5])
     mine = nall[z]
     stacked = jnp.concatenate([mine[:, 256 * k:256 * (k + 1)] for k in range(NZ)], axis=0)
@@ -304,21 +352,11 @@
     tbuf[0:ROWS, 0:4] = new_max
     nmax_ref[...] = tbuf[...].T[0:4, 0:ROWS]
 
-    for d in (1, 7, 2, 6, 3, 5, 4):
-        zs = zpeer(d)
-        arrived(nall.at[zs, :, other], f_r.at[zs])
-    arrived(wfull.at[:, 0:15], one_r.at[4])
-
-    every = nn_dot(nall[...].reshape(NZ * ROWS, D), wfull[...].reshape(D, 128))
-    res[...] = every.astype(BF16).reshape(NZ, ROWS, 128)
-
-    def p_send(d):
-        zt = zpeer(d)
-        return push(res.at[zt], proj.at[z], one_s.at[7], one_r.at[7], (zt, y, x, c))
-
-    for d in ZOFF:
-        p_send(d).start()
-    proj[z] = res[z]
+    for side in (1, -1):
+        zs = zpeer(NZ - 2 * side)
+        arrived(wofb.at[zs], e_r.at[zs])
+        eb_relay(side)
+
     arrived(proj.at[0:7], one_r.at[7])
 
     lane = lax.broadcasted_iota(jnp.int32, (ROWS, 128), 1)
@@ -382,7 +420,17 @@
         cell[:, at] = (scaled * hg[:, at] * jax.nn.sigmoid(gate)).astype(BF16)
 
     arrived(wof.at[:, 0:15], one_r.at[6])
-    p_my[...] = nt_dot(cell[...], wof[...].reshape(D, 256)).astype(BF16)
+    for d in (1, 7, 3, 5, 4):
+        zs = zpeer(d)
+        if d == 4:
+            arrived(wofb.at[zs, 0:8], e_r.at[zs])
+            arrived(wofb.at[zs, 8:16], e4_r)
+        else:
+            arrived(wofb.at[zs], e_r.at[zs])
+    p_my[...] = (
+        nt_dot(cell[:, 0:128], wof[...].reshape(D, 128))
+        + nt_dot(cell[:, 128:256], wofb[...].reshape(D, 128))
+    ).astype(BF16)
     swap = push(p_my, p_ot, one_s.at[8], one_r.at[8], partner)
     swap.start()
     swap.wait_recv()
@@ -515,6 +563,10 @@
     left(wfull.at[:, 0:15], one_s.at[4])
     left(gt.at[0:15], one_s.at[5])
     left(wof.at[:, 0:15], one_s.at[6])
+    left(wofb.at[0, 0:15], one_s.at[15])
+    left(wofb.at[0:4], one_s.at[16])
+    left(wofb.at[0:2], one_s.at[17])
+    left(wofb.at[0:1], one_s.at[18])
     left(res.at[0:7], one_s.at[7])
     left(p_my, one_s.at[8])
     left(outt.at[0:127], one_s.at[9])
@@ -580,8 +632,9 @@
             buf((16, 128)),
             buf((NZ, NP, 16, 128)),
             buf((NP, 16, 128)),
-            buf((NZ, 16, 256)),
-            buf((NZ, NP, 16, 256)),
+            buf((NZ, 16, 128)),
+            buf((NZ, NP, 16, 128)),
+            buf((NZ, NP, 16, 128)),
             buf((NZ, ROWS, 128)),
             buf((NZ, ROWS, 128)),
             buf((128, 128), F32),
@@ -612,12 +665,13 @@
             buf((128, 16, 128)),
             buf((128, 16, 128)),
             dma((len(args),)),
+            dma((2, NZ)),
             dma((NZ,)),
             dma,
             dma,
             dma((NZ,)),
-            dma((15,)),
-            dma((15,)),
+            dma((19,)),
+            dma((19,)),
             dma((NZ,)),
             dma,
             dma((NZ,)),

time: 78.7 us -> 74.8 us (0.950)
  Pallas kernels: 77.9 us -> 74.1 us
    pallas_call x1, Pallas kernels: 75.8 us -> 72 us  [fused(): pl.pallas_call(fused_kernel, name='layer', out_shape=tuple((pltpu.VMEM(sh...]
where the time goes in v5:
time: 74.8 us
  Pallas kernels  74.1 us (99%)
    pallas_call x1, Pallas kernels, fused(): pl.pallas_call(fused_kernel, name='layer', out_shape=tuple((pltpu.VMEM(sh...  72 us
    pallas_call x1, Pallas kernels, stored(): pl.pallas_call(store_kernel, name='store', out_shape=tuple((jax.ShapeDtyp...  2.15 us

profile of v5, /device:TPU:1, one launch (start us, length us, event | category | flops | bytes accessed | tf_op | source)
XLA Modules:
  0.0 74.8 jit_solution(12346377225740847136)
XLA Ops:
  0.6 72.0 %layer.1 = (bf16[32,2048]{1,0:T(8,128)(2,1)S(1)}, f32[8192,64]{1,0:T(8,128)S(1)}, f32[32,4,64]{2,1,0:T(4,128)S(1)}, f32[4,32]{1,0:T(4,128)S(1)}) custom-call(bf16[32,2048]{1,0:T(8,128)(2,1)} %tok_h.1, f32[1,2048]{1,0:T(1,128)} %bitcast.19, bf16[16,256]{1,0:T(8,128)(2,1)} %wq_h.1, bf16[16,256]{1,0:T(8,128)(2,1)} %wk_h.1, bf16[16,256]{1,0:T(8,128)(2,1)} %wv_h.1, ...), custom_call_target="tpu_custom_call" | custom-call | tf_op jit(solution)/shard_map/layer/pallas_call | solution.py:619
  72.6 2.1 %store.1 = (bf16[32,2048]{1,0:T(8,128)(2,1)}, f32[8192,64]{1,0:T(8,128)}, f32[32,4,64]{2,1,0:T(4,128)}, f32[4,32]{1,0:T(4,128)}) custom-call(bf16[32,2048]{1,0:T(8,128)(2,1)S(1)} %get-tuple-element.12.refs_0_, f32[8192,64]{1,0:T(8,128)S(1)} %get-tuple-element.13.refs_1_, f32[32,4,64]{2,1,0:T(4,128)S(1)} %get-tuple-element.14.refs_2_, ...), custom_call_target="tpu_custom_call" | custom-call | tf_op jit(solution)/shard_map/store/pallas_call | solution.py:599

commit v6 on v5

--- a/solution.py
+++ b/solution.py
@@ -49,7 +49,6 @@
 
 
 ZOFF = (4, 3, 5, 2, 6, 1, 7)
-JOFF = (10, 9, 11, 6, 14, 2, 8, 5, 7, 13, 15, 1, 3, 4, 12, 0)
 OUTS = (((ROWS, D), BF16), ((ROWS * 256, 64), F32), ((ROWS, 4, 64), F32), ((4, ROWS), F32))
 
 
@@ -91,8 +90,6 @@
 
         lax.fori_loop(lo, hi, step, 0)
 
-    spots = [ppeer(j) for j in range(NP)]
-
     def planes(body):
         def step(i, carry):
             body(i, zpeer(4 + (1 - 2 * (i % 2)) * ((i + 1) // 2)))
@@ -100,14 +97,21 @@
 
         lax.fori_loop(0, NZ, step, 0)
 
-    def send_plane(i, zt, send):
-        for j in JOFF:
-            yt, xt, yxt = spots[j]
-            copy = send((zt, yt, xt, c), zt * NP + yxt)
-            if j:
-                copy.start()
-            else:
-                pl.when(i < NZ - 1)(copy.start)
+    def far_first(a):
+        return 2 + (1 - 2 * (a % 2)) * ((a + 1) // 2)
+
+    def send_all(send):
+        def place(k):
+            yt, xt = (y + far_first(k // NX)) % NY, (x + far_first(k % NX)) % NX
+            for off in (*ZOFF, 0):
+                zt = zpeer(off)
+                copy = send((zt, yt, xt, c), zt * NP + yt * NX + xt)
+                if off:
+                    copy.start()
+                else:
+                    pl.when(k < NP - 1)(copy.start)
+
+        loop(0, NP, place)
 
     barrier = pltpu.get_barrier_semaphore()
 
@@ -456,9 +460,9 @@
     def dispatch(i, zt):
         rows = nn_dot(amat[plane256(zt), :], xr).astype(BF16)
         outt[plane16(zt)] = rows.reshape(NP, 16, 128)
-        send_plane(i, zt, d_send)
 
     planes(dispatch)
+    send_all(d_send)
     rcv[c, me] = outt[me]
 
     def write_one(b):
@@ -533,9 +537,9 @@
 
     def give_back(i, zt):
         back[plane16(zt)] = yf[plane256(zt), :].astype(BF16).reshape(NP, 16, 128)
-        send_plane(i, zt, b_send)
 
     planes(give_back)
+    send_all(b_send)
     ret[me] = back[me]
 
     weighted = jnp.zeros((512, 128), F32)

time: 74.8 us -> 77.2 us (1.032)
  Pallas kernels: 74.1 us -> 76.5 us
    pallas_call x1, Pallas kernels: 72 us -> 74.4 us  [fused(): pl.pallas_call(fused_kernel, name='layer', out_shape=tuple((pltpu.VMEM(sh...]
where the time goes in v6:
time: 77.2 us
  Pallas kernels  76.5 us (99%)
    pallas_call x1, Pallas kernels, fused(): pl.pallas_call(fused_kernel, name='layer', out_shape=tuple((pltpu.VMEM(sh...  74.4 us
    pallas_call x1, Pallas kernels, stored(): pl.pallas_call(store_kernel, name='store', out_shape=tuple((jax.ShapeDtyp...  2.15 us

profile of v6, /device:TPU:1, one launch (start us, length us, event | category | flops | bytes accessed | tf_op | source)
XLA Modules:
  0.0 77.2 jit_solution(7445391331012331809)
XLA Ops:
  0.6 74.4 %layer.1 = (bf16[32,2048]{1,0:T(8,128)(2,1)S(1)}, f32[8192,64]{1,0:T(8,128)S(1)}, f32[32,4,64]{2,1,0:T(4,128)S(1)}, f32[4,32]{1,0:T(4,128)S(1)}) custom-call(bf16[32,2048]{1,0:T(8,128)(2,1)} %tok_h.1, f32[1,2048]{1,0:T(1,128)} %bitcast.19, bf16[16,256]{1,0:T(8,128)(2,1)} %wq_h.1, bf16[16,256]{1,0:T(8,128)(2,1)} %wk_h.1, bf16[16,256]{1,0:T(8,128)(2,1)} %wv_h.1, ...), custom_call_target="tpu_custom_call" | custom-call | tf_op jit(solution)/shard_map/layer/pallas_call | solution.py:623
  75.0 2.1 %store.1 = (bf16[32,2048]{1,0:T(8,128)(2,1)}, f32[8192,64]{1,0:T(8,128)}, f32[32,4,64]{2,1,0:T(4,128)}, f32[4,32]{1,0:T(4,128)}) custom-call(bf16[32,2048]{1,0:T(8,128)(2,1)S(1)} %get-tuple-element.12.refs_0_, f32[8192,64]{1,0:T(8,128)S(1)} %get-tuple-element.13.refs_1_, f32[32,4,64]{2,1,0:T(4,128)S(1)} %get-tuple-element.14.refs_2_, ...), custom_call_target="tpu_custom_call" | custom-call | tf_op jit(solution)/shard_map/store/pallas_call | solution.py:603
